TPU v7x, 256 devices: a whole 4x4x8 slice. The times are simulated.
256 devices in a mesh: ep: 64 (over z, x, core), tp: 4 (over y).
Axes of the slice: x: 4, y: 4, z: 8, core: 2. Of those that a mesh axis runs over, the one named last changes fastest.
Arguments:
- head_inputs_unfiltered: bfloat16 [8192, 4096], P('ep', 'tp'), may hold values from -6 to 6
- group_write_vectors: bfloat16 [8192, 512], P('ep', 'tp'), may hold values from -6 to 6
- group_read_vectors: bfloat16 [8192, 512], P('ep', 'tp'), may hold values from -6 to 6
- output_gate_inputs: bfloat16 [8192, 4096], P('ep', 'tp'), may hold values from -6 to 6
- step_preactivation: float32 [64, 8192], P('tp', 'ep'), may hold values from -3.2 to 3.6
- extra_decay_logs: float32 [64, 8192], P('tp', 'ep'), may hold values from -0.7 to 0
- head_decay_logs: float32 [64], P('tp'), may hold values from -16 to -2.7
- head_filter_taps: bfloat16 [4, 4096], P(None, 'tp'), may hold values from -3 to 3
- write_filter_taps: bfloat16 [4, 512], P(None, 'tp'), may hold values from -3 to 3
- read_filter_taps: bfloat16 [4, 512], P(None, 'tp'), may hold values from -3 to 3
- grouped_norm_gain: float32 [4096], P('tp'), may hold values from 0.1 to 1.9
- mixer_output_weight: bfloat16 [4096, 2048], P('tp'), may hold values from -0.09375 to 0.09375
- expert_input_rows: bfloat16 [32768, 2048], P(('ep', 'tp')), may hold values from -6 to 6
- expert_norm_gain: float32 [2048], replicated, may hold values from 0.1 to 1.9
- routes: int32 [32768, 2], P(('ep', 'tp')), may hold values from 0 to 63, all different within a row; in each aligned block of 128 rows (0 to 127, 128 to 255, ...) at most 6 rows name the same one
- router_chosen_scores: bfloat16 [32768, 2], P(('ep', 'tp')), may hold values from 0.049804688 to 1
- routed_gate_weight: bfloat16 [64, 2048, 1024], P('ep', None, 'tp'), may hold values from -0.125 to 0.125
- routed_up_weight: bfloat16 [64, 2048, 1024], P('ep', None, 'tp'), may hold values from -0.125 to 0.125
- routed_down_weight: bfloat16 [64, 1024, 2048], P('ep', 'tp'), may hold values from -0.1875 to 0.1875
- shared_gate_weight: bfloat16 [2048, 512], P(None, 'tp'), may hold values from -0.125 to 0.125
- shared_up_weight: bfloat16 [2048, 512], P(None, 'tp'), may hold values from -0.125 to 0.125
- shared_down_weight: bfloat16 [512, 2048], P('tp'), may hold values from -0.25 to 0.25
Outputs:
- mixer_result: bfloat16 [8192, 2048], P(('ep', 'tp'))
- moe_result: bfloat16 [32768, 2048], P(('ep', 'tp'))
Inputs may be any that keep to these rules, and one draw needn't show every extreme that they name: `routes`: within the 128 rows of one device no expert is named more than 6 times; a row names 2 different experts.
All inputs are finite; a program needn't handle non-finite values.
Results may differ from a plain program's by a relative error of at most 0.0095.
Values may be sent and summed in bfloat16 or wider, within the bound.
No kernel may reach another device: no remote copies, remote signals or barrier semaphores. Data moves between devices by JAX's collectives and lax.ppermute only.
A program may use at most 128 MiB of HBM per device.

v0:
```python
import functools

import jax
import jax.numpy as jnp
from jax import lax
from jax.experimental import pallas as pl
from jax.experimental.pallas import tpu as pltpu
from jax.sharding import Mesh
from jax.sharding import PartitionSpec as P


HEAD_DIM = 64
STATE = 128
LANE = 128
EP = ("ep_0", "ep_1", "ep_2")
EP_TP = ("ep_0", "ep_1", "ep_2", "tp")

eps_norm = 1e-06
route_scale = 2.5
highest = lax.Precision.HIGHEST
f32 = jnp.float32
bf16 = jnp.bfloat16


MIB = 1024 * 1024


def shift(value, axis, by, wrap):
    devices = lax.axis_size(axis)
    if wrap:
        pairs = [(i, (i + by) % devices) for i in range(devices)]
    else:
        pairs = [(i, i + by) for i in range(devices) if 0 <= i + by < devices]
    return lax.ppermute(value, axis, pairs)


def call(body, outs, scratch, mib):
    return pl.pallas_call(
        body,
        out_shape=outs,
        scratch_shapes=list(scratch),
        compiler_params=pltpu.CompilerParams(vmem_limit_bytes=mib * MIB),
    )


def dispatch_body(capacity, experts, x_ref, gain_ref, routes_ref, normed_ref, out_ref, scr):
    rows, width = x_ref.shape
    x = x_ref[...].astype(f32)
    scale = lax.rsqrt(jnp.mean(x * x, axis=-1, keepdims=True) + eps_norm)
    normed_ref[...] = (x * scale * gain_ref[...]).astype(bf16)
    first = routes_ref[0:1, :]
    second = routes_ref[1:2, :]
    names = lax.broadcasted_iota(jnp.int32, (experts, rows), 0)
    hit0 = (names == first).astype(f32)
    hit1 = (names == second).astype(f32)
    earlier = (
        lax.broadcasted_iota(jnp.int32, (rows, rows), 0)
        < lax.broadcasted_iota(jnp.int32, (rows, rows), 1)
    ).astype(bf16)
    before = jnp.dot((hit0 + hit1).astype(bf16), earlier, preferred_element_type=f32)
    slot0 = first * capacity + jnp.sum(before * hit0, axis=0, keepdims=True).astype(jnp.int32)
    slot1 = second * capacity + jnp.sum(before * hit1, axis=0, keepdims=True).astype(jnp.int32)
    slots = experts * capacity
    place = lax.broadcasted_iota(jnp.int32, (slots, rows), 0)
    pick = ((place == slot0) | (place == slot1)).astype(bf16)
    pieces = width // LANE
    for k in range(0, pieces, 2):
        part = jnp.dot(
            pick, normed_ref[:, k * LANE : (k + 2) * LANE], preferred_element_type=f32
        )
        scr[pl.ds(k, slots, stride=pieces), :] = part[:, :LANE]
        scr[pl.ds(k + 1, slots, stride=pieces), :] = part[:, LANE:]
    out_ref[...] = scr[...].astype(bf16)


def expert_hidden(x, gate, up):
    gate_value = jnp.dot(x, gate, preferred_element_type=f32)
    up_value = jnp.dot(x, up, preferred_element_type=f32)
    return (gate_value * jax.nn.sigmoid(gate_value) * up_value).astype(bf16)


def expert_first_body(in_ref, w0, w1, w2, rows_ref, sum_ref, scr):
    slots, width = rows_ref.shape
    pieces = width // LANE
    scr[...] = in_ref[...].astype(f32)
    for k in range(pieces):
        rows_ref[:, k * LANE : (k + 1) * LANE] = scr[pl.ds(k, slots, stride=pieces), :].astype(bf16)
    x = rows_ref[...]
    units = w0.shape[1]
    hidden = [expert_hidden(x, w[:width, :], w[width : 2 * width, :]) for w in (w0, w1, w2)]
    for j in range(width // units):
        rows = slice(2 * width + j * units, 2 * width + (j + 1) * units)
        sum_ref[:, j * units : (j + 1) * units] = (
            jnp.dot(hidden[0], w0[rows, :], preferred_element_type=f32)
            + jnp.dot(hidden[1], w1[rows, :], preferred_element_type=f32)
            + jnp.dot(hidden[2], w2[rows, :], preferred_element_type=f32)
        )


def expert_last_body(rows_ref, sum_ref, wa, wb, out_ref, scr):
    slots, width = rows_ref.shape
    pieces = width // LANE
    units = wa.shape[1]
    edge = wa.shape[0]
    x = rows_ref[...]
    gate_value = jnp.dot(x, wa[:width, :], preferred_element_type=f32)
    up_value = jnp.dot(x[:, : edge - width], wa[width:, :], preferred_element_type=f32) + jnp.dot(
        x[:, edge - width :], wb[: 2 * width - edge, :], preferred_element_type=f32
    )
    hidden = (gate_value * jax.nn.sigmoid(gate_value) * up_value).astype(bf16)
    for k in range(0, pieces, 2):
        row = 2 * width - edge + k // 2 * units
        part = sum_ref[:, k * LANE : (k + 2) * LANE] + jnp.dot(
            hidden, wb[row : row + units, :], preferred_element_type=f32
        )
        scr[pl.ds(k, slots, stride=pieces), :] = part[:, :LANE]
        scr[pl.ds(k + 1, slots, stride=pieces), :] = part[:, LANE:]
    out_ref[...] = scr[...].astype(bf16)


def shared_body(core_ref, n_ref, *refs):
    out_ref = refs[-1]
    held = refs[:-1]
    core = core_ref[0]
    half = n_ref.shape[1] // 2
    mine = n_ref[:, pl.ds(pl.multiple_of(core * half, LANE), half)]
    other = n_ref[:, pl.ds(pl.multiple_of((1 - core) * half, LANE), half)]
    count = len(held) // 2
    low = jnp.zeros((n_ref.shape[0], half), f32)
    high = jnp.zeros((n_ref.shape[0], half), f32)
    for q in range(count):
        a = held[q]
        b = held[count + q]
        gate_value = jnp.dot(mine, a[:half, :], preferred_element_type=f32) + jnp.dot(
            other, b[:half, :], preferred_element_type=f32
        )
        up_value = jnp.dot(mine, a[half : 2 * half, :], preferred_element_type=f32) + jnp.dot(
            other, b[half : 2 * half, :], preferred_element_type=f32
        )
        hidden = (gate_value * jax.nn.sigmoid(gate_value) * up_value).astype(bf16)
        blocks = half // LANE
        low += jnp.concatenate(
            [
                jnp.dot(
                    hidden,
                    a[2 * half + j * LANE : 2 * half + (j + 1) * LANE, :],
                    preferred_element_type=f32,
                )
                for j in range(blocks)
            ],
            axis=1,
        )
        high += jnp.concatenate(
            [
                jnp.dot(
                    hidden,
                    b[2 * half + j * LANE : 2 * half + (j + 1) * LANE, :],
                    preferred_element_type=f32,
                )
                for j in range(blocks)
            ],
            axis=1,
        )
    out_ref[:, pl.ds(pl.multiple_of(core * half, LANE), half)] = low
    out_ref[:, pl.ds(pl.multiple_of((1 - core) * half, LANE), half)] = high


def combine_body(capacity, experts, in_ref, routes_ref, scores_ref, shared_ref, out_ref, scr):
    rows, width = out_ref.shape
    pieces = width // LANE
    slots = experts * capacity
    scr[...] = in_ref[...].astype(f32)
    first = routes_ref[:, 0:1]
    second = routes_ref[:, 1:2]
    names = lax.broadcasted_iota(jnp.int32, (rows, experts), 1)
    hit0 = (names == first).astype(f32)
    hit1 = (names == second).astype(f32)
    earlier = (
        lax.broadcasted_iota(jnp.int32, (rows, rows), 1)
        < lax.broadcasted_iota(jnp.int32, (rows, rows), 0)
    ).astype(bf16)
    before = jnp.dot(earlier, (hit0 + hit1).astype(bf16), preferred_element_type=f32)
    slot0 = first * capacity + jnp.sum(before * hit0, axis=1, keepdims=True).astype(jnp.int32)
    slot1 = second * capacity + jnp.sum(before * hit1, axis=1, keepdims=True).astype(jnp.int32)
    place = lax.broadcasted_iota(jnp.int32, (rows, slots), 1)
    pick = jnp.concatenate(
        [(place == slot0).astype(bf16), (place == slot1).astype(bf16)], axis=0
    )
    scores = scores_ref[...].astype(f32)
    weights = scores / jnp.sum(scores, axis=1, keepdims=True) * route_scale
    w0 = weights[:, 0:1]
    w1 = weights[:, 1:2]
    for k in range(0, pieces, 2):
        both = jnp.concatenate(
            [
                scr[pl.ds(k, slots, stride=pieces), :].astype(bf16),
                scr[pl.ds(k + 1, slots, stride=pieces), :].astype(bf16),
            ],
            axis=1,
        )
        got = jnp.dot(pick, both, preferred_element_type=f32)
        cols = slice(k * LANE, (k + 2) * LANE)
        out_ref[:, cols] = (
            got[:rows] * w0 + got[rows:] * w1 + shared_ref[:, cols]
        ).astype(bf16)


def conv_silu(values, weights):
    taps = weights.shape[0]
    length = values.shape[0] - taps + 1
    running_sum = jnp.zeros((length, values.shape[1]), f32)
    for offset in range(taps):
        running_sum = running_sum + weights[offset].astype(f32) * values[
            offset : offset + length
        ].astype(f32)
    return jax.nn.silu(running_sum)


def mixer_rows(
    head_inputs_unfiltered,
    group_write_vectors,
    group_read_vectors,
    output_gate_inputs,
    step_preactivation,
    extra_decay_logs,
    head_decay_logs,
    head_filter_taps,
    write_filter_taps,
    read_filter_taps,
    grouped_norm_gain,
):
    row_total, head_chans = head_inputs_unfiltered.shape
    taps = head_filter_taps.shape[0]
    write_chans = group_write_vectors.shape[1]
    heads = step_preactivation.shape[0]
    groups = write_chans // STATE
    per_group = heads // groups
    ep_count = lax.axis_size(EP)
    step = jax.nn.softplus(step_preactivation)
    log_rate = -jnp.exp(head_decay_logs)[:, None] * step + extra_decay_logs
    upto = jnp.triu(jnp.ones((row_total, row_total), f32))
    cumulative = jnp.dot(log_rate, upto, precision=highest)
    device_decay = cumulative[:, -1]
    tail_rows = jnp.concatenate(
        [
            head_inputs_unfiltered[row_total - taps + 1 :],
            group_write_vectors[row_total - taps + 1 :],
            group_read_vectors[row_total - taps + 1 :],
        ],
        axis=1,
    )
    earlier = shift(tail_rows, EP, 1, False)
    padded_heads = jnp.concatenate([earlier[:, :head_chans], head_inputs_unfiltered], axis=0)
    padded_write = jnp.concatenate(
        [earlier[:, head_chans : head_chans + write_chans], group_write_vectors], axis=0
    )
    padded_read = jnp.concatenate(
        [earlier[:, head_chans + write_chans :], group_read_vectors], axis=0
    )
    head_values = conv_silu(padded_heads, head_filter_taps).reshape(
        row_total, groups, per_group, HEAD_DIM
    )
    write_values = conv_silu(padded_write, write_filter_taps).reshape(row_total, groups, STATE)
    read_values = conv_silu(padded_read, read_filter_taps).reshape(row_total, groups, STATE)
    cum = cumulative.reshape(groups, per_group, row_total)
    weighted = head_values * jnp.transpose(
        step.reshape(groups, per_group, row_total), (2, 0, 1)
    )[..., None]
    to_end = jnp.exp(cum[..., -1:] - cum)
    device_state = jnp.einsum(
        "sgn,sgep->gepn",
        write_values,
        weighted * jnp.transpose(to_end, (2, 0, 1))[..., None],
        precision=highest,
    )
    state_rows = heads * HEAD_DIM // ep_count
    split_decay = []
    rest = jnp.repeat(device_decay, ep_count // heads)
    for _ in range(3):
        piece = lax.reduce_precision(rest, 8, 7)
        split_decay.append(piece)
        rest = rest - piece
    decay_lanes = jnp.stack(split_decay, axis=1)
    decay_block = jnp.pad(decay_lanes[:, None, :], ((0, 0), (0, 15), (0, STATE - 3)))
    sent = jnp.concatenate(
        [
            device_state.reshape(ep_count, state_rows, STATE).astype(bf16),
            decay_block.astype(bf16),
        ],
        axis=1,
    )
    arrived = lax.all_to_all(sent, EP, 0, 0, tiled=True)
    held = arrived[:, :state_rows]
    decays = jnp.sum(arrived[:, state_rows, :3].astype(f32), axis=1)
    order = jnp.arange(ep_count)
    strictly = order[None, :] < order[:, None]
    ends = jnp.dot((order[None, :] <= order[:, None]).astype(f32), decays, precision=highest)
    carry = jnp.exp(
        jnp.where(strictly, (ends - decays)[:, None] - ends[None, :], -jnp.inf)
    )
    entering = jnp.dot(
        carry, held.reshape(ep_count, -1).astype(f32), precision=highest
    ).astype(bf16)
    returned = lax.all_to_all(entering.reshape(ep_count, state_rows, STATE), EP, 0, 0, tiled=True)
    incoming = returned.reshape(groups, per_group, HEAD_DIM, STATE).astype(f32)
    lower = jnp.tril(jnp.ones((row_total, row_total), bool))
    within = jnp.exp(jnp.where(lower, cum[..., :, None] - cum[..., None, :], -jnp.inf))
    affinity = jnp.einsum("lgn,sgn->gls", read_values, write_values, precision=highest)
    local_part = jnp.einsum(
        "gels,sgep->lgep", affinity[:, None] * within, weighted, precision=highest
    )
    carried_part = (
        jnp.einsum("lgn,gepn->lgep", read_values, incoming, precision=highest)
        * jnp.transpose(jnp.exp(cum), (2, 0, 1))[..., None]
    )
    scan_out = (local_part + carried_part).reshape(row_total, groups, per_group * HEAD_DIM)
    gate_values = jax.nn.silu(output_gate_inputs.astype(f32)).reshape(
        row_total, groups, per_group * HEAD_DIM
    )
    gated_rows = scan_out * gate_values
    gated_rows = gated_rows * lax.rsqrt(
        jnp.mean(gated_rows * gated_rows, axis=-1, keepdims=True) + eps_norm
    )
    return (gated_rows.reshape(row_total, head_chans) * grouped_norm_gain).astype(bf16)


def layer(
    head_inputs_unfiltered,
    group_write_vectors,
    group_read_vectors,
    output_gate_inputs,
    step_preactivation,
    extra_decay_logs,
    head_decay_logs,
    head_filter_taps,
    write_filter_taps,
    read_filter_taps,
    grouped_norm_gain,
    mixer_output_weight,
    expert_input_rows,
    expert_norm_gain,
    routes,
    router_chosen_scores,
    routed_gate_weight,
    routed_up_weight,
    routed_down_weight,
    shared_gate_weight,
    shared_up_weight,
    shared_down_weight,
):
    tp_count = lax.axis_size("tp")
    ep_count = lax.axis_size(EP)
    core = lax.axis_index("ep_2")
    rows, width = expert_input_rows.shape
    experts = routed_gate_weight.shape[0] * ep_count
    capacity = 3 * rows * routes.shape[1] // (2 * experts)
    slots = experts * capacity
    pieces = width // LANE

    units = routed_gate_weight.shape[2]
    own = jnp.concatenate(
        [
            routed_gate_weight[0],
            routed_up_weight[0],
            routed_down_weight[0]
            .reshape(units, width // units, units)
            .transpose(1, 0, 2)
            .reshape(width, units),
        ],
        axis=0,
    )
    from_low = shift(own, "tp", 1, True)
    from_high = shift(own, "tp", -1, True)

    normed, sent_rows = call(
        functools.partial(dispatch_body, capacity, experts),
        (
            jax.ShapeDtypeStruct((rows, width), bf16),
            jax.ShapeDtypeStruct((slots * pieces, LANE), bf16),
        ),
        [pltpu.VMEM((slots * pieces, LANE), f32)],
        16,
    )(expert_input_rows, expert_norm_gain[None, :], routes.T)
    arrived = lax.all_to_all(
        sent_rows.reshape(experts, capacity * pieces, LANE), EP, 0, 0, tiled=True
    ).reshape(slots * pieces, LANE)

    edge = own.shape[0] // 2
    far_a = shift(from_low[:edge], "tp", 1, True)
    far_b = shift(from_high[edge:], "tp", -1, True)

    mixer_normed = mixer_rows(
        head_inputs_unfiltered,
        group_write_vectors,
        group_read_vectors,
        output_gate_inputs,
        step_preactivation,
        extra_decay_logs,
        head_decay_logs,
        head_filter_taps,
        write_filter_taps,
        read_filter_taps,
        grouped_norm_gain,
    )
    mix_rows = mixer_normed.shape[0]
    mix_term = jnp.dot(mixer_normed, mixer_output_weight, preferred_element_type=f32).astype(bf16)
    tp_index = lax.axis_index("tp")
    block = mix_rows // tp_count
    mix_total = None
    for by in range(tp_count):
        target = (tp_index + by) % tp_count
        part = lax.dynamic_slice_in_dim(mix_term, target * block, block, 0)
        if by:
            part = shift(part, "tp", by, True)
        part = part.astype(f32)
        mix_total = part if mix_total is None else mix_total + part
    mixer_result = mix_total.astype(bf16)

    expert_rows, expert_sum = call(
        expert_first_body,
        (
            jax.ShapeDtypeStruct((slots, width), bf16),
            jax.ShapeDtypeStruct((slots, width), f32),
        ),
        [pltpu.VMEM((slots * pieces, LANE), f32)],
        32,
    )(arrived, own, from_low, from_high)
    sent_back = call(
        expert_last_body,
        jax.ShapeDtypeStruct((slots * pieces, LANE), bf16),
        [pltpu.VMEM((slots * pieces, LANE), f32)],
        24,
    )(expert_rows, expert_sum, far_a, far_b)
    returned = lax.all_to_all(
        sent_back.reshape(experts, capacity * pieces, LANE), EP, 0, 0, tiled=True
    ).reshape(slots * pieces, LANE)

    cut = width // 2
    shared_own = jnp.concatenate(
        [
            lax.dynamic_slice_in_dim(shared_gate_weight, core * cut, cut, 0),
            lax.dynamic_slice_in_dim(shared_up_weight, core * cut, cut, 0),
            lax.dynamic_slice_in_dim(shared_down_weight, core * cut, cut, 1)
            .reshape(LANE, cut // LANE, LANE)
            .transpose(1, 0, 2)
            .reshape(cut, LANE),
        ],
        axis=0,
    )
    shared_low = shift(shared_own, "tp", 1, True)
    shared_high = shift(shared_own, "tp", -1, True)
    middle = shared_own.shape[0] // 2
    shared_far = [
        shift(shared_low[:middle], "tp", 1, True),
        shift(shared_high[middle:], "tp", -1, True),
    ]
    shared_far = jnp.concatenate(shared_far, axis=0)
    shared_mine = [shared_own, shared_low, shared_high, shared_far]
    shared_other = [shift(w, "ep_2", 1, True) for w in shared_mine]
    shared_sum = pl.pallas_call(
        shared_body,
        out_shape=jax.ShapeDtypeStruct((rows, width), f32),
        in_specs=[pl.BlockSpec(memory_space=pltpu.SMEM)] + [pl.BlockSpec(memory_space=pltpu.VMEM)] * 9,
        compiler_params=pltpu.CompilerParams(vmem_limit_bytes=16 * MIB),
        name="shared",
    )(core[None].astype(jnp.int32), normed, *shared_mine, *shared_other)

    moe_result = call(
        functools.partial(combine_body, capacity, experts),
        jax.ShapeDtypeStruct((rows, width), bf16),
        [pltpu.VMEM((slots * pieces, LANE), f32)],
        16,
    )(returned, routes, router_chosen_scores, shared_sum)
    return (mixer_result, moe_result)


def solution(mesh):
    split = Mesh(mesh.devices.reshape(8, 4, 2, mesh.shape["tp"]), ("ep_0", "ep_1", "ep_2", "tp"))
    placed = (
        P(EP, "tp"),
        P(EP, "tp"),
        P(EP, "tp"),
        P(EP, "tp"),
        P("tp", EP),
        P("tp", EP),
        P("tp"),
        P(None, "tp"),
        P(None, "tp"),
        P(None, "tp"),
        P("tp"),
        P("tp", None),
        P(EP_TP, None),
        P(),
        P(EP_TP, None),
        P(EP_TP, None),
        P(EP, None, "tp"),
        P(EP, None, "tp"),
        P(EP, "tp", None),
        P(None, "tp"),
        P(None, "tp"),
        P("tp", None),
    )
    return jax.shard_map(
        layer,
        mesh=split,
        in_specs=placed,
        out_specs=(P(EP_TP, None), P(EP_TP, None)),
        check_vma=False,
    )
```

profile of v0, /device:TPU:2, one launch (start us, length us, event | category | flops | bytes accessed | tf_op | source)
XLA Modules:
  0.0 203.8 jit_solution(5072042985889227945)
XLA Ops:
  0.7 1.7 copy.60
  2.7 1.8 pad_maximum_fusion.w0
  4.5 1.6 collective-permute-start.4
  6.0 1.7 collective-permute-start.5
  8.7 1.9 collective-permute-start
  12.0 5.1 %collective-permute-done = bf16[3,1280]{0,1:T(8,128)(2,1)S(1)} collective-permute-done((bf16[3,1280]{0,1:T(8,128)(2,1)S(1)}, bf16[3,1280]{0,1:T(8,128)(2,1)S(1)}, u32[]{:S(2)}, u32[]{:S(2)}) %collective-permute-start) | collective-permute-done | bytes 7712 | tf_op jit(solution)/shard_map/ppermute | solution.py:34
  17.2 1.1 divide_multiply_fusion
  19.0 0.9 fusion.12
  19.9 12.9 %all-to-all-start = ((bf16[64,32,128]{2,1,0:T(8,128)(2,1)}), bf16[64,32,128]{2,1,0:T(8,128)(2,1)S(1)}, u32[]{:S(2)}, u32[]{:S(2)}) async-start(bf16[64,32,128]{2,1,0:T(8,128)(2,1)} %fusion.12), calls=%async_computation | async-start | bytes 1048576 | tf_op jit(solution)/shard_map/all_to_all | solution.py:292
  32.8 1.4 shard_map.221
  34.2 1.1 copy-done.3
  35.4 0.8 copy-done.4
  36.2 14.1 %all-to-all-done = bf16[64,32,128]{2,1,0:T(8,128)(2,1)S(1)} async-done(((bf16[64,32,128]{2,1,0:T(8,128)(2,1)}), bf16[64,32,128]{2,1,0:T(8,128)(2,1)S(1)}, u32[]{:S(2)}, u32[]{:S(2)}) %all-to-all-start) | async-done | bytes 524320 | tf_op jit(solution)/shard_map/all_to_all | solution.py:292
  51.1 5.8 %all-to-all-start.2 = ((bf16[64,96,128]{2,1,0:T(8,128)(2,1)}), bf16[64,96,128]{2,1,0:T(8,128)(2,1)S(1)}, u32[]{:S(2)}, u32[]{:S(2)}) async-start(bf16[64,96,128]{2,1,0:T(8,128)(2,1)} %bitcast.115), calls=%async_computation.2 | async-start | bytes 3145728 | tf_op jit(solution)/shard_map/all_to_all | solution.py:384
  57.0 18.9 %collective-permute-done.4.w1 = bf16[6144,256]{1,0:T(8,128)(2,1)} collective-permute-done((bf16[6144,256]{1,0:T(8,128)(2,1)}, bf16[6144,256]{1,0:T(8,128)(2,1)}, u32[]{:S(2)}, u32[]{:S(2)}) %collective-permute-start.4) | collective-permute-done | bytes 3145760 | tf_op jit(solution)/shard_map/ppermute | solution.py:34
  75.9 2.7 %slice.159 = bf16[3072,256]{1,0:T(8,128)(2,1)} slice(bf16[6144,256]{1,0:T(8,128)(2,1)} %collective-permute-done.4.w1), slice={[0:3072], [0:256]} | slice | bytes 3145728 | tf_op jit(solution)/shard_map/slice | solution.py:389
  78.9 2.7 %slice.160 = bf16[3072,256]{1,0:T(8,128)(2,1)} slice(bf16[6144,256]{1,0:T(8,128)(2,1)} %collective-permute-done.5.w2), slice={[3072:6144], [0:256]} | slice | bytes 3145728 | tf_op jit(solution)/shard_map/slice | solution.py:390
  81.5 2.9 %collective-permute-start.7 = (bf16[3072,256]{1,0:T(8,128)(2,1)}, bf16[3072,256]{1,0:T(8,128)(2,1)}, u32[]{:S(2)}, u32[]{:S(2)}) collective-permute-start(bf16[3072,256]{1,0:T(8,128)(2,1)} %slice.160), channel_id=1, source_target_pairs={{0,3},{1,0},{2,1},{3,2},{4,7},{5,4},{6,5},{7,6},{8,11},{9,8},{10,9... | collective-permute-start | bytes 4718600 | tf_op jit(solution)/shard_map/ppermute | solution.py:34
  84.7 0.9 copy.54
  85.6 1.1 constant_dynamic-slice_fusion.1
  86.6 1.0 pad_maximum_fusion.1.refs_0_
  87.7 1.2 slice.158
  88.9 1.5 fusion.34
  91.7 5.3 %all-to-all-done.2 = bf16[64,96,128]{2,1,0:T(8,128)(2,1)S(1)} async-done(((bf16[64,96,128]{2,1,0:T(8,128)(2,1)}), bf16[64,96,128]{2,1,0:T(8,128)(2,1)S(1)}, u32[]{:S(2)}, u32[]{:S(2)}) %all-to-all-start.2) | async-done | bytes 1572896 | tf_op jit(solution)/shard_map/all_to_all | solution.py:384
  97.0 6.9 %all-to-all-start.1 = ((bf16[64,16,128]{2,1,0:T(8,128)(2,1)}), bf16[64,16,128]{2,1,0:T(8,128)(2,1)}, u32[]{:S(2)}, u32[]{:S(2)}) async-start(bf16[64,16,128]{2,1,0:T(8,128)(2,1)} %bitcast.124), calls=%async_computation.1 | async-start | bytes 524288 | tf_op jit(solution)/shard_map/all_to_all | solution.py:304
  103.9 3.1 %collective-permute-start.9 = (bf16[3072,128]{1,0:T(8,128)(2,1)S(1)}, bf16[3072,128]{1,0:T(8,128)(2,1)}, u32[]{:S(2)}, u32[]{:S(2)}) collective-permute-start(bf16[3072,128]{1,0:T(8,128)(2,1)S(1)} %pad_maximum_fusion.1.refs_0_), channel_id=1, source_target_pairs={{0,3},{1,0},{2,1},{3,2},{4,7},{5,4},{6,5},{7,6},{8,11},{9,8},{10,9... | collective-permute-start | bytes 2359304 | tf_op jit(solution)/shard_map/ppermute | solution.py:34
  107.0 1.8 copy.51
  109.5 22.8 %collective-permute-done.8.refs_1_ = bf16[3072,128]{1,0:T(8,128)(2,1)} collective-permute-done((bf16[3072,128]{1,0:T(8,128)(2,1)S(1)}, bf16[3072,128]{1,0:T(8,128)(2,1)}, u32[]{:S(2)}, u32[]{:S(2)}) %collective-permute-start.8) | collective-permute-done | bytes 786464 | tf_op jit(solution)/shard_map/ppermute | solution.py:34
  132.3 1.8 slice.161
  134.0 8.5 %shard_map.222 = (bf16[384,2048]{1,0:T(8,128)(2,1)S(1)}, f32[384,2048]{1,0:T(8,128)S(1)}) custom-call(bf16[6144,128]{1,0:T(8,128)(2,1)S(1)} %bitcast.114, bf16[6144,256]{1,0:T(8,128)(2,1)} %pad_maximum_fusion.w0, bf16[6144,256]{1,0:T(8,128)(2,1)} %collective-permute-done.4.w1, bf16[6144,256]{1,0:T(8,128)(2,1)} %collective-permute-done.5.w2), custom_call_target="tpu_custom_call" | custom-call | tf_op jit(solution)/shard_map/pallas_call | solution.py:419
  142.6 5.3 %shard_map.223 = bf16[6144,128]{1,0:T(8,128)(2,1)} custom-call(bf16[384,2048]{1,0:T(8,128)(2,1)S(1)} %get-tuple-element.7.rows_ref, f32[384,2048]{1,0:T(8,128)S(1)} %get-tuple-element.8.sum_ref, bf16[3072,256]{1,0:T(8,128)(2,1)} %collective-permute-done.6.wa, bf16[3072,256]{1,0:T(8,128)(2,1)} %collective-permute-done.7.wb), custom_call_target="tpu_custom_call" | custom-call | tf_op jit(solution)/shard_map/pallas_call | solution.py:428
  147.8 12.1 %all-to-all-start.3 = ((bf16[64,96,128]{2,1,0:T(8,128)(2,1)}), bf16[64,96,128]{2,1,0:T(8,128)(2,1)S(1)}, u32[]{:S(2)}, u32[]{:S(2)}) async-start(bf16[64,96,128]{2,1,0:T(8,128)(2,1)} %bitcast.44), calls=%async_computation.3 | async-start | bytes 3145728 | tf_op jit(solution)/shard_map/all_to_all | solution.py:434
  160.0 0.9 divide_multiply_fusion.2
  161.2 1.1 slice.162
  162.3 3.3 %collective-permute-start.11 = (bf16[1536,128]{1,0:T(8,128)(2,1)S(1)}, bf16[1536,128]{1,0:T(8,128)(2,1)S(1)}, u32[]{:S(2)}, u32[]{:S(2)}) collective-permute-start(bf16[1536,128]{1,0:T(8,128)(2,1)S(1)} %slice.162), channel_id=1, source_target_pairs={{0,3},{1,0},{2,1},{3,2},{4,7},{5,4},{6,5},{7,6},{8,11},{9,8},{10,9... | collective-permute-start | bytes 1179656 | tf_op jit(solution)/shard_map/ppermute | solution.py:34
  166.1 1.8 constant_dynamic-update-slice_fusion.1
  167.9 1.3 fusion.1
  169.3 2.2 %fusion = f32[128,1,16,64]{0,3,2,1:T(8,128)S(1)} fusion(f32[128,1,16,64]{0,3,2,1:T(8,128)S(1)} %fusion.1, f32[16,128]{1,0:T(8,128)S(1)} %fusion.28, f32[128,128]{1,0:T(8,128)S(1)} %fusion.59, pred[128,128]{1,0:T(8,128)(4,1)S(1)} %iota_compare_fusion.2, f32[128,16,64]{0,2,1:T(8,128)S(1)} %bitcast.119, f32[128,16]{0,1:T(8,128)S(1)} %fusion.46), kind=kOutput, calls=%fused_computation.5 | convolution fusion | flops 202375168 | bytes 1671168 | tf_op jit(solution)/shard_map/gels,sgep->lgep/dot_general | solution.py:309
  171.4 1.2 multiply_reduce_fusion
  172.6 0.8 convolution_convert_fusion
  175.3 4.5 %collective-permute-done.3 = bf16[32,2048]{1,0:T(8,128)(2,1)S(1)} collective-permute-done((bf16[32,2048]{1,0:T(8,128)(2,1)S(1)}, bf16[32,2048]{1,0:T(8,128)(2,1)S(1)}, u32[]{:S(2)}, u32[]{:S(2)}) %collective-permute-start.3) | collective-permute-done | bytes 131104 | tf_op jit(solution)/shard_map/ppermute | solution.py:34
  179.9 6.3 %collective-permute-done.2 = bf16[32,2048]{1,0:T(8,128)(2,1)S(1)} collective-permute-done((bf16[32,2048]{1,0:T(8,128)(2,1)S(1)}, bf16[32,2048]{1,0:T(8,128)(2,1)S(1)}, u32[]{:S(2)}, u32[]{:S(2)}) %collective-permute-start.2) | collective-permute-done | bytes 131104 | tf_op jit(solution)/shard_map/ppermute | solution.py:34
  186.5 5.9 %collective-permute-done.1 = bf16[32,2048]{1,0:T(8,128)(2,1)S(1)} collective-permute-done((bf16[32,2048]{1,0:T(8,128)(2,1)S(1)}, bf16[32,2048]{1,0:T(8,128)(2,1)S(1)}, u32[]{:S(2)}, u32[]{:S(2)}) %collective-permute-start.1) | collective-permute-done | bytes 131104 | tf_op jit(solution)/shard_map/ppermute | solution.py:34
  192.4 1.6 add_convert_fusion
  194.1 1.1 copy-done.2
  195.2 1.0 copy-done.5
  196.3 4.9 %shared.1.shared_ref = f32[128,2048]{1,0:T(8,128)S(1)} custom-call(s32[1]{0:T(128)} %bitcast.46.core_ref, bf16[128,2048]{1,0:T(8,128)(2,1)S(1)} %copy-done.5, bf16[3072,128]{1,0:T(8,128)(2,1)S(1)} %copy-done.2, bf16[3072,128]{1,0:T(8,128)(2,1)} %collective-permute-done.8.refs_1_, bf16[3072,128]{1,0:T(8,128)(2,1)} %collective-permute-done.9.refs_2_, ...), custom_call_target="tpu_custom_call" | custom-call | tf_op jit(solution)/shard_map/shared/pallas_call | solution.py:460
  201.2 2.7 %shard_map.224 = bf16[128,2048]{1,0:T(8,128)(2,1)} custom-call(bf16[6144,128]{1,0:T(8,128)(2,1)S(1)} %bitcast.113, s32[128,2]{1,0:T(8,128)S(1)} %copy.55.routes_ref, bf16[128,2]{1,0:T(8,128)(2,1)S(1)} %copy.56.scores_ref, f32[128,2048]{1,0:T(8,128)S(1)} %shared.1.shared_ref), custom_call_target="tpu_custom_call" | custom-call | tf_op jit(solution)/shard_map/pallas_call | solution.py:468
  (109 shorter events, 9.7 us)
Async XLA Ops:
  0.6 83.8 %copy-start = (bf16[128,2048]{1,0:T(8,128)(2,1)S(1)}, bf16[128,2048]{1,0:T(8,128)(2,1)}, u32[]{:S(2)}) copy-start(bf16[128,2048]{1,0:T(8,128)(2,1)} %param.43) | copy-start | bytes 1572868
  0.6 1.9 copy-start.12
  0.7 1.9 copy-start.13
  2.6 5.8 %copy-start.15 = (bf16[128,128]{1,0:T(8,128)(2,1)S(1)}, bf16[128,128]{1,0:T(8,128)(2,1)}, u32[]{:S(2)}) copy-start(bf16[128,128]{1,0:T(8,128)(2,1)} %param.23) | copy-start | bytes 98308
  2.6 5.8 %copy-start.14 = (bf16[128,1024]{1,0:T(8,128)(2,1)S(1)}, bf16[128,1024]{1,0:T(8,128)(2,1)}, u32[]{:S(2)}) copy-start(bf16[128,1024]{1,0:T(8,128)(2,1)} %param.22) | copy-start | bytes 786436
  2.6 8.0 %copy-start.24 = (f32[16]{0:T(128)S(1)}, f32[16]{0:T(128)}, u32[]{:S(2)}) copy-start(f32[16]{0:T(128)} %param.28) | copy-start | bytes 196
  2.6 8.0 %copy-start.18 = (f32[16,128]{1,0:T(8,128)S(1)}, f32[16,128]{1,0:T(8,128)}, u32[]{:S(2)}) copy-start(f32[16,128]{1,0:T(8,128)} %param.26) | copy-start | bytes 24580
  2.6 8.1 %copy-start.23 = (f32[16,128]{1,0:T(8,128)S(1)}, f32[16,128]{1,0:T(8,128)}, u32[]{:S(2)}) copy-start(f32[16,128]{1,0:T(8,128)} %param.27) | copy-start | bytes 24580
  2.6 8.7 %copy-start.17 = (bf16[4,1024]{1,0:T(4,128)(2,1)S(1)}, bf16[4,1024]{1,0:T(4,128)(2,1)}, u32[]{:S(2)}) copy-start(bf16[4,1024]{1,0:T(4,128)(2,1)} %param.29) | copy-start | bytes 24580
  2.7 9.0 %copy-start.20 = (bf16[4,128]{1,0:T(4,128)(2,1)S(1)}, bf16[4,128]{1,0:T(4,128)(2,1)}, u32[]{:S(2)}) copy-start(bf16[4,128]{1,0:T(4,128)(2,1)} %param.30) | copy-start | bytes 3076
  4.5 71.4 %collective-permute-start.4 = (bf16[6144,256]{1,0:T(8,128)(2,1)}, bf16[6144,256]{1,0:T(8,128)(2,1)}, u32[]{:S(2)}, u32[]{:S(2)}) collective-permute-start(bf16[6144,256]{1,0:T(8,128)(2,1)} %pad_maximum_fusion.w0), channel_id=1, source_target_pairs={{0,1},{1,2},{2,3},{3,0},{4,5},{5,6},{6,7},{7,4},{8,9},{9,10},{10,1... | collective-permute-start | bytes 9437192 | tf_op jit(solution)/shard_map/ppermute | solution.py:34
  6.0 72.8 %collective-permute-start.5 = (bf16[6144,256]{1,0:T(8,128)(2,1)}, bf16[6144,256]{1,0:T(8,128)(2,1)}, u32[]{:S(2)}, u32[]{:S(2)}) collective-permute-start(bf16[6144,256]{1,0:T(8,128)(2,1)} %pad_maximum_fusion.w0), channel_id=1, source_target_pairs={{0,3},{1,0},{2,1},{3,2},{4,7},{5,4},{6,5},{7,6},{8,11},{9,8},{10,9... | collective-permute-start | bytes 9437192 | tf_op jit(solution)/shard_map/ppermute | solution.py:34
  8.7 8.4 %collective-permute-start = (bf16[3,1280]{0,1:T(8,128)(2,1)S(1)}, bf16[3,1280]{0,1:T(8,128)(2,1)S(1)}, u32[]{:S(2)}, u32[]{:S(2)}) collective-permute-start(bf16[3,1280]{0,1:T(8,128)(2,1)S(1)} %copy.45), channel_id=1, source_target_pairs={{0,4},{4,8},{8,12},{12,16},{16,20},{20,24},{24,28},{28,32},{32,36}... | collective-permute-start | bytes 23048 | tf_op jit(solution)/shard_map/ppermute | solution.py:34
  11.3 21.4 %copy-start.6 = (bf16[128,2048]{1,0:T(8,128)(2,1)S(1)}, bf16[128,2048]{1,0:T(8,128)(2,1)}, u32[]{:S(2)}) copy-start(bf16[128,2048]{1,0:T(8,128)(2,1)} %x_ref.1) | copy-start | bytes 1572868
  11.4 21.4 %copy-start.7 = (f32[2048]{0:T(1024)S(1)}, f32[2048]{0:T(1024)}, u32[]{:S(2)}) copy-start(f32[2048]{0:T(1024)} %param.35) | copy-start | bytes 24580
  11.4 21.4 %copy-start.8 = (s32[128,2]{0,1:T(2,128)S(1)}, s32[128,2]{0,1:T(2,128)}, u32[]{:S(2)}) copy-start(s32[128,2]{0,1:T(2,128)} %param.36) | copy-start | bytes 3076
  19.9 30.4 %all-to-all-start = ((bf16[64,32,128]{2,1,0:T(8,128)(2,1)}), bf16[64,32,128]{2,1,0:T(8,128)(2,1)S(1)}, u32[]{:S(2)}, u32[]{:S(2)}) async-start(bf16[64,32,128]{2,1,0:T(8,128)(2,1)} %fusion.12), calls=%async_computation | async-start | bytes 1048576 | tf_op jit(solution)/shard_map/all_to_all | solution.py:292
  34.2 1.1 copy-start.3
  35.4 0.8 copy-start.4
  50.3 0.8 copy-start.11
  51.1 45.9 %all-to-all-start.2 = ((bf16[64,96,128]{2,1,0:T(8,128)(2,1)}), bf16[64,96,128]{2,1,0:T(8,128)(2,1)S(1)}, u32[]{:S(2)}, u32[]{:S(2)}) async-start(bf16[64,96,128]{2,1,0:T(8,128)(2,1)} %bitcast.115), calls=%async_computation.2 | async-start | bytes 3145728 | tf_op jit(solution)/shard_map/all_to_all | solution.py:384
  78.5 64.0 %collective-permute-start.6 = (bf16[3072,256]{1,0:T(8,128)(2,1)}, bf16[3072,256]{1,0:T(8,128)(2,1)}, u32[]{:S(2)}, u32[]{:S(2)}) collective-permute-start(bf16[3072,256]{1,0:T(8,128)(2,1)} %slice.159), channel_id=1, source_target_pairs={{0,1},{1,2},{2,3},{3,0},{4,5},{5,6},{6,7},{7,4},{8,9},{9,10},{10,1... | collective-permute-start | bytes 4718600 | tf_op jit(solution)/shard_map/ppermute | solution.py:34
  81.5 61.0 %collective-permute-start.7 = (bf16[3072,256]{1,0:T(8,128)(2,1)}, bf16[3072,256]{1,0:T(8,128)(2,1)}, u32[]{:S(2)}, u32[]{:S(2)}) collective-permute-start(bf16[3072,256]{1,0:T(8,128)(2,1)} %slice.160), channel_id=1, source_target_pairs={{0,3},{1,0},{2,1},{3,2},{4,7},{5,4},{6,5},{7,6},{8,11},{9,8},{10,9... | collective-permute-start | bytes 4718600 | tf_op jit(solution)/shard_map/ppermute | solution.py:34
  84.5 24.3 %copy-start.21 = (bf16[4,128]{1,0:T(4,128)(2,1)S(1)}, bf16[4,128]{1,0:T(4,128)(2,1)}, u32[]{:S(2)}) copy-start(bf16[4,128]{1,0:T(4,128)(2,1)} %param.31) | copy-start | bytes 3076
  87.6 54.9 %copy-start.1 = (bf16[3072,128]{1,0:T(8,128)(2,1)}, bf16[3072,128]{1,0:T(8,128)(2,1)S(1)}, u32[]{:S(2)}) copy-start(bf16[3072,128]{1,0:T(8,128)(2,1)S(1)} %pad_maximum_fusion.1.refs_0_) | copy-start | bytes 2359300
  87.6 44.6 %collective-permute-start.8 = (bf16[3072,128]{1,0:T(8,128)(2,1)S(1)}, bf16[3072,128]{1,0:T(8,128)(2,1)}, u32[]{:S(2)}, u32[]{:S(2)}) collective-permute-start(bf16[3072,128]{1,0:T(8,128)(2,1)S(1)} %pad_maximum_fusion.1.refs_0_), channel_id=1, source_target_pairs={{0,1},{1,2},{2,3},{3,0},{4,5},{5,6},{6,7},{7,4},{8,9},{9,10},{10,1... | collective-permute-start | bytes 2359304 | tf_op jit(solution)/shard_map/ppermute | solution.py:34
  97.0 50.9 %all-to-all-start.1 = ((bf16[64,16,128]{2,1,0:T(8,128)(2,1)}), bf16[64,16,128]{2,1,0:T(8,128)(2,1)}, u32[]{:S(2)}, u32[]{:S(2)}) async-start(bf16[64,16,128]{2,1,0:T(8,128)(2,1)} %bitcast.124), calls=%async_computation.1 | async-start | bytes 524288 | tf_op jit(solution)/shard_map/all_to_all | solution.py:304
  103.9 57.3 %collective-permute-start.9 = (bf16[3072,128]{1,0:T(8,128)(2,1)S(1)}, bf16[3072,128]{1,0:T(8,128)(2,1)}, u32[]{:S(2)}, u32[]{:S(2)}) collective-permute-start(bf16[3072,128]{1,0:T(8,128)(2,1)S(1)} %pad_maximum_fusion.1.refs_0_), channel_id=1, source_target_pairs={{0,3},{1,0},{2,1},{3,2},{4,7},{5,4},{6,5},{7,6},{8,11},{9,8},{10,9... | collective-permute-start | bytes 2359304 | tf_op jit(solution)/shard_map/ppermute | solution.py:34
  107.0 87.1 %collective-permute-start.12 = (bf16[3072,128]{1,0:T(8,128)(2,1)S(1)}, bf16[3072,128]{1,0:T(8,128)(2,1)}, u32[]{:S(2)}, u32[]{:S(2)}) collective-permute-start(bf16[3072,128]{1,0:T(8,128)(2,1)S(1)} %pad_maximum_fusion.1.refs_0_), channel_id=1, source_target_pairs={{0,4},{4,0},{1,5},{5,1},{2,6},{6,2},{3,7},{7,3},{8,12},{12,8},{9,1... | collective-permute-start | bytes 2359304 | tf_op jit(solution)/shard_map/ppermute | solution.py:34
  134.0 32.1 %collective-permute-start.10 = (bf16[1536,128]{1,0:T(8,128)(2,1)}, bf16[1536,128]{1,0:T(8,128)(2,1)}, u32[]{:S(2)}, u32[]{:S(2)}) collective-permute-start(bf16[1536,128]{1,0:T(8,128)(2,1)} %slice.161), channel_id=1, source_target_pairs={{0,1},{1,2},{2,3},{3,0},{4,5},{5,6},{6,7},{7,4},{8,9},{9,10},{10,1... | collective-permute-start | bytes 1179656 | tf_op jit(solution)/shard_map/ppermute | solution.py:34
  147.8 12.2 %copy-start.16 = (bf16[128,128]{1,0:T(8,128)(2,1)S(1)}, bf16[128,128]{1,0:T(8,128)(2,1)}, u32[]{:S(2)}) copy-start(bf16[128,128]{1,0:T(8,128)(2,1)} %param.24) | copy-start | bytes 98308
  147.8 53.3 %all-to-all-start.3 = ((bf16[64,96,128]{2,1,0:T(8,128)(2,1)}), bf16[64,96,128]{2,1,0:T(8,128)(2,1)S(1)}, u32[]{:S(2)}, u32[]{:S(2)}) async-start(bf16[64,96,128]{2,1,0:T(8,128)(2,1)} %bitcast.44), calls=%async_computation.3 | async-start | bytes 3145728 | tf_op jit(solution)/shard_map/all_to_all | solution.py:434
  160.0 12.6 %copy-start.9 = (bf16[1024,2048]{1,0:T(8,128)(2,1)S(1)}, bf16[1024,2048]{1,0:T(8,128)(2,1)}, u32[]{:S(2)}) copy-start(bf16[1024,2048]{1,0:T(8,128)(2,1)} %param.33) | copy-start | bytes 12582916
  160.0 12.6 %copy-start.19 = (f32[1024]{0:T(1024)S(1)}, f32[1024]{0:T(1024)}, u32[]{:S(2)}) copy-start(f32[1024]{0:T(1024)} %param.32) | copy-start | bytes 12292
  162.3 12.2 %collective-permute-start.11 = (bf16[1536,128]{1,0:T(8,128)(2,1)S(1)}, bf16[1536,128]{1,0:T(8,128)(2,1)S(1)}, u32[]{:S(2)}, u32[]{:S(2)}) collective-permute-start(bf16[1536,128]{1,0:T(8,128)(2,1)S(1)} %slice.162), channel_id=1, source_target_pairs={{0,3},{1,0},{2,1},{3,2},{4,7},{5,4},{6,5},{7,6},{8,11},{9,8},{10,9... | collective-permute-start | bytes 1179656 | tf_op jit(solution)/shard_map/ppermute | solution.py:34
  165.6 28.5 %collective-permute-start.13 = (bf16[3072,128]{1,0:T(8,128)(2,1)}, bf16[3072,128]{1,0:T(8,128)(2,1)}, u32[]{:S(2)}, u32[]{:S(2)}) collective-permute-start(bf16[3072,128]{1,0:T(8,128)(2,1)} %collective-permute-done.8.refs_1_), channel_id=1, source_target_pairs={{0,4},{4,0},{1,5},{5,1},{2,6},{6,2},{3,7},{7,3},{8,12},{12,8},{9,1... | collective-permute-start | bytes 2359304 | tf_op jit(solution)/shard_map/ppermute | solution.py:34
  165.6 28.5 %collective-permute-start.14 = (bf16[3072,128]{1,0:T(8,128)(2,1)}, bf16[3072,128]{1,0:T(8,128)(2,1)}, u32[]{:S(2)}, u32[]{:S(2)}) collective-permute-start(bf16[3072,128]{1,0:T(8,128)(2,1)} %collective-permute-done.9.refs_2_), channel_id=1, source_target_pairs={{0,4},{4,0},{1,5},{5,1},{2,6},{6,2},{3,7},{7,3},{8,12},{12,8},{9,1... | collective-permute-start | bytes 2359304 | tf_op jit(solution)/shard_map/ppermute | solution.py:34
  172.6 13.8 %copy-start.22 = (bf16[128,2]{0,1:T(2,128)(2,1)S(1)}, bf16[128,2]{0,1:T(2,128)(2,1)}, u32[]{:S(2)}) copy-start(bf16[128,2]{0,1:T(2,128)(2,1)} %param.37) | copy-start | bytes 1540
  173.5 0.8 copy-start.10
  174.3 5.5 %collective-permute-start.3 = (bf16[32,2048]{1,0:T(8,128)(2,1)S(1)}, bf16[32,2048]{1,0:T(8,128)(2,1)S(1)}, u32[]{:S(2)}, u32[]{:S(2)}) collective-permute-start(bf16[32,2048]{1,0:T(8,128)(2,1)S(1)} %get-tuple-element.13), channel_id=1, source_target_pairs={{0,3},{1,0},{2,1},{3,2},{4,7},{5,4},{6,5},{7,6},{8,11},{9,8},{10,9... | collective-permute-start | bytes 393224 | tf_op jit(solution)/shard_map/ppermute | solution.py:34
  175.3 18.8 %collective-permute-start.15 = (bf16[3072,128]{1,0:T(8,128)(2,1)}, bf16[3072,128]{1,0:T(8,128)(2,1)}, u32[]{:S(2)}, u32[]{:S(2)}) collective-permute-start(bf16[3072,128]{1,0:T(8,128)(2,1)} %constant_dynamic-update-slice_fusion.refs_3_), channel_id=1, source_target_pairs={{0,4},{4,0},{1,5},{5,1},{2,6},{6,2},{3,7},{7,3},{8,12},{12,8},{9,1... | collective-permute-start | bytes 2359304 | tf_op jit(solution)/shard_map/ppermute | solution.py:34
  179.8 6.5 %collective-permute-start.2 = (bf16[32,2048]{1,0:T(8,128)(2,1)S(1)}, bf16[32,2048]{1,0:T(8,128)(2,1)S(1)}, u32[]{:S(2)}, u32[]{:S(2)}) collective-permute-start(bf16[32,2048]{1,0:T(8,128)(2,1)S(1)} %get-tuple-element.14), channel_id=1, source_target_pairs={{0,2},{1,3},{2,0},{3,1},{4,6},{5,7},{6,4},{7,5},{8,10},{9,11},{10,... | collective-permute-start | bytes 393224 | tf_op jit(solution)/shard_map/ppermute | solution.py:34
  186.3 6.2 %collective-permute-start.1 = (bf16[32,2048]{1,0:T(8,128)(2,1)S(1)}, bf16[32,2048]{1,0:T(8,128)(2,1)S(1)}, u32[]{:S(2)}, u32[]{:S(2)}) collective-permute-start(bf16[32,2048]{1,0:T(8,128)(2,1)S(1)} %get-tuple-element.12), channel_id=1, source_target_pairs={{0,1},{1,2},{2,3},{3,0},{4,5},{5,6},{6,7},{7,4},{8,9},{9,10},{10,1... | collective-permute-start | bytes 393224 | tf_op jit(solution)/shard_map/ppermute | solution.py:34
  194.1 1.1 copy-start.2
  195.2 1.0 copy-start.5
where the time goes:
time: 205 us; the launch traced here: 204 us
  waiting for transfers between devices  83 us (40%)
  starting transfers between devices  53.6 us (26%)
  local copies, waits for them, and re-layouts  26.6 us (13%)
  Pallas kernels  22.7 us (11%)
  other arithmetic  10.8 us (5%)
  matrix products  5.99 us (3%)
    ppermute x16, waiting for transfers between devices, shift(): return lax.ppermute(value, axis, pairs)  63.5 us
    ppermute x16, starting transfers between devices, shift(): return lax.ppermute(value, axis, pairs)  15.8 us
    all_to_all x1, waiting for transfers between devices, mixer_rows(): arrived = lax.all_to_all(sent, EP, 0, 0, tiled=True)  14.1 us
    all_to_all x1, starting transfers between devices, mixer_rows(): arrived = lax.all_to_all(sent, EP, 0, 0, tiled=True)  12.9 us
    unnamed x58, local copies, waits for them, and re-layouts  12.4 us
    all_to_all x1, starting transfers between devices, layer(): lax.all_to_all(sent_back.reshape(experts, capacity * pieces, LANE), EP, 0...  12.1 us
    pallas_call x1, Pallas kernels, layer(): call(expert_first_body, (jax.ShapeDtypeStruct((slots, width), bf16), jax....  8.49 us
    all_to_all x1, starting transfers between devices, mixer_rows(): lax.all_to_all(entering.reshape(ep_count, state_rows, STATE), EP, 0, 0, t...  6.94 us
  transfers between devices with their start and end apart: 20, of which 8 were waited for; matrix products, arithmetic and copies ran while one was open for 17% of the time, Pallas kernels for 10%

commit v1 on v0

v1 whole, which is shorter than its diff:
```python
import functools

import jax
import jax.numpy as jnp
from jax import lax
from jax.experimental import pallas as pl
from jax.experimental.pallas import tpu as pltpu
from jax.sharding import Mesh
from jax.sharding import PartitionSpec as P


HEAD_DIM = 64
STATE = 128
LANE = 128
EP = ("ep_0", "ep_1", "ep_2")
EP_TP = ("ep_0", "ep_1", "ep_2", "tp")

eps_norm = 1e-06
route_scale = 2.5
highest = lax.Precision.HIGHEST
f32 = jnp.float32
bf16 = jnp.bfloat16


MIB = 1024 * 1024


def shift(value, axis, by, wrap):
    devices = lax.axis_size(axis)
    if wrap:
        pairs = [(i, (i + by) % devices) for i in range(devices)]
    else:
        pairs = [(i, i + by) for i in range(devices) if 0 <= i + by < devices]
    return lax.ppermute(value, axis, pairs)


def call(body, outs, scratch, mib):
    return pl.pallas_call(
        body,
        out_shape=outs,
        scratch_shapes=list(scratch),
        compiler_params=pltpu.CompilerParams(vmem_limit_bytes=mib * MIB),
    )


def place_rows(capacity, experts, chunk_rows, x_ref, gain_ref, routes_ref, normed_ref, scr):
    rows, width = x_ref.shape
    x = x_ref[...].astype(f32)
    scale = lax.rsqrt(jnp.mean(x * x, axis=-1, keepdims=True) + eps_norm)
    normed_ref[...] = (x * scale * gain_ref[...]).astype(bf16)
    first = routes_ref[0:1, :]
    second = routes_ref[1:2, :]
    names = lax.broadcasted_iota(jnp.int32, (experts, rows), 0)
    hit0 = (names == first).astype(f32)
    hit1 = (names == second).astype(f32)
    earlier = (
        lax.broadcasted_iota(jnp.int32, (rows, rows), 0)
        < lax.broadcasted_iota(jnp.int32, (rows, rows), 1)
    ).astype(bf16)
    before = jnp.dot((hit0 + hit1).astype(bf16), earlier, preferred_element_type=f32)
    slot0 = first + experts * jnp.sum(before * hit0, axis=0, keepdims=True).astype(jnp.int32)
    slot1 = second + experts * jnp.sum(before * hit1, axis=0, keepdims=True).astype(jnp.int32)
    slots = experts * capacity
    place = lax.broadcasted_iota(jnp.int32, (slots, rows), 0)
    pick = ((place == slot0) | (place == slot1)).astype(bf16)
    pieces = width // LANE
    for k in range(0, pieces, 2):
        part = jnp.dot(
            pick, normed_ref[:, k * LANE : (k + 2) * LANE], preferred_element_type=f32
        )
        for r in range(capacity):
            own = part[r * experts : (r + 1) * experts, :]
            row = r * pieces + k
            scr[pl.ds(row, experts, stride=chunk_rows), :] = own[:, :LANE]
            scr[pl.ds(row + 1, experts, stride=chunk_rows), :] = own[:, LANE:]


def expert_hidden(x, gate, up):
    gate_value = jnp.dot(x, gate, preferred_element_type=f32)
    up_value = jnp.dot(x, up, preferred_element_type=f32)
    return (gate_value * jax.nn.sigmoid(gate_value) * up_value).astype(bf16)


def expert_first_body(
    capacity, chunk_rows, in_ref, g0, u0, d0, g1, u1, d1a, d1b, g2, u2, d2a, d2b, rows_ref, sum_ref, scr
):
    slots, width = rows_ref.shape
    pieces = width // LANE
    sources = slots // capacity
    scr[...] = in_ref[...].astype(f32)
    for r in range(capacity):
        for k in range(pieces):
            got = scr[pl.ds(r * pieces + k, sources, stride=chunk_rows), :]
            rows_ref[r * sources : (r + 1) * sources, k * LANE : (k + 1) * LANE] = got.astype(bf16)
    x = rows_ref[...]
    hidden = [expert_hidden(x, g[...], u[...]) for g, u in ((g0, u0), (g1, u1), (g2, u2))]
    half = d1a.shape[0]
    for k in range(0, pieces, 2):
        cols = slice(k * LANE, (k + 2) * LANE)
        sum_ref[:, cols] = (
            jnp.dot(hidden[0], d0[:, cols], preferred_element_type=f32)
            + jnp.dot(hidden[1][:, :half], d1a[:, cols], preferred_element_type=f32)
            + jnp.dot(hidden[1][:, half:], d1b[:, cols], preferred_element_type=f32)
            + jnp.dot(hidden[2][:, :half], d2a[:, cols], preferred_element_type=f32)
            + jnp.dot(hidden[2][:, half:], d2b[:, cols], preferred_element_type=f32)
        )


def expert_hidden_body(rows_ref, g, u, hidden_ref):
    hidden_ref[...] = expert_hidden(rows_ref[...], g[...], u[...])


def expert_last_body(capacity, hidden_ref, sum_ref, da, db, out_ref, scr):
    slots, width = sum_ref.shape
    pieces = width // LANE
    hidden = hidden_ref[...]
    half = da.shape[0]
    for k in range(0, pieces, 2):
        cols = slice(k * LANE, (k + 2) * LANE)
        part = (
            sum_ref[:, cols]
            + jnp.dot(hidden[:, :half], da[:, cols], preferred_element_type=f32)
            + jnp.dot(hidden[:, half:], db[:, cols], preferred_element_type=f32)
        )
        sources = slots // capacity
        for r in range(capacity):
            own = part[r * sources : (r + 1) * sources, :]
            row = r * pieces + k
            scr[pl.ds(row, sources, stride=capacity * pieces), :] = own[:, :LANE]
            scr[pl.ds(row + 1, sources, stride=capacity * pieces), :] = own[:, LANE:]
    out_ref[...] = scr[...].astype(bf16)


def shared_pack_body(core_ref, gate_ref, up_ref, down_ref, out_ref):
    width, chans = gate_ref.shape
    half = chans // 2
    core = core_ref[0]
    gate = gate_ref[...].astype(f32)
    up = up_ref[...].astype(f32)
    left = lax.broadcasted_iota(jnp.int32, (width, chans), 1) < half
    first = jnp.where(left, gate, pltpu.roll(up, half, 1))
    second = jnp.where(left, pltpu.roll(gate, half, 1), up)
    out_ref[:width, :] = jnp.where(core == 0, first, second).astype(bf16)
    rows = pl.multiple_of(core * half, half)
    for j in range(width // LANE):
        out_ref[width + j * half : width + (j + 1) * half, :] = down_ref[
            pl.ds(rows, half), j * LANE : (j + 1) * LANE
        ]


def shared_body(mine_ref, other_ref, own, low, high, far, sum_ref, send_ref):
    rows, width = mine_ref.shape
    x = jnp.concatenate([mine_ref[...], other_ref[...]], axis=0)
    lanes = lax.broadcasted_iota(jnp.int32, (2 * rows, LANE), 1) < LANE // 2
    packs = (own, low, high, far)
    hidden = []
    for pair in (packs[:2], packs[2:]):
        halves = []
        for pack in pair:
            both = jnp.dot(x, pack[:width, :], preferred_element_type=f32)
            up_value = pltpu.roll(both, LANE // 2, 1)
            halves.append(both * jax.nn.sigmoid(both) * up_value)
        hidden.append(jnp.where(lanes, halves[0], pltpu.roll(halves[1], LANE // 2, 1)))
    hidden = jnp.concatenate(hidden, axis=1).astype(bf16)
    units = LANE // 2
    for j in range(0, width // LANE, 2):
        down = jnp.concatenate(
            [
                jnp.concatenate(
                    [pack[width + i * units : width + (i + 1) * units, :] for pack in packs], axis=0
                )
                for i in (j, j + 1)
            ],
            axis=1,
        )
        part = jnp.dot(hidden, down, preferred_element_type=f32)
        cols = slice(j * LANE, (j + 2) * LANE)
        sum_ref[:, cols] = part[:rows]
        send_ref[:, cols] = part[rows:].astype(bf16)


def combine_body(
    capacity, experts, in_ref, routes_ref, scores_ref, shared_ref, other_ref, out_ref, scr
):
    rows, width = out_ref.shape
    pieces = width // LANE
    slots = experts * capacity
    scr[...] = in_ref[...].astype(f32)
    first = routes_ref[:, 0:1]
    second = routes_ref[:, 1:2]
    names = lax.broadcasted_iota(jnp.int32, (rows, experts), 1)
    hit0 = (names == first).astype(f32)
    hit1 = (names == second).astype(f32)
    earlier = (
        lax.broadcasted_iota(jnp.int32, (rows, rows), 1)
        < lax.broadcasted_iota(jnp.int32, (rows, rows), 0)
    ).astype(bf16)
    before = jnp.dot(earlier, (hit0 + hit1).astype(bf16), preferred_element_type=f32)
    slot0 = first * capacity + jnp.sum(before * hit0, axis=1, keepdims=True).astype(jnp.int32)
    slot1 = second * capacity + jnp.sum(before * hit1, axis=1, keepdims=True).astype(jnp.int32)
    place = lax.broadcasted_iota(jnp.int32, (rows, slots), 1)
    pick = jnp.concatenate(
        [(place == slot0).astype(bf16), (place == slot1).astype(bf16)], axis=0
    )
    scores = scores_ref[...].astype(f32)
    weights = scores / jnp.sum(scores, axis=1, keepdims=True) * route_scale
    w0 = weights[:, 0:1]
    w1 = weights[:, 1:2]
    for k in range(0, pieces, 2):
        both = jnp.concatenate(
            [
                scr[pl.ds(k, slots, stride=pieces), :].astype(bf16),
                scr[pl.ds(k + 1, slots, stride=pieces), :].astype(bf16),
            ],
            axis=1,
        )
        got = jnp.dot(pick, both, preferred_element_type=f32)
        cols = slice(k * LANE, (k + 2) * LANE)
        out_ref[:, cols] = (
            got[:rows] * w0
            + got[rows:] * w1
            + (shared_ref[:, cols] + other_ref[:, cols].astype(f32))
        ).astype(bf16)


def conv_silu(x_ref, tail, taps_ref, pad_ref):
    rows, chans = x_ref.shape
    taps = taps_ref.shape[0]
    start = 8 - taps + 1
    pad_ref[8 : 8 + rows, :chans] = x_ref[...].astype(f32)
    pad_ref[start:8, :chans] = tail.astype(f32)
    weights = taps_ref[...].astype(f32)
    total = weights[0:1, :] * pad_ref[start : start + rows, :chans]
    for j in range(1, taps):
        total = total + weights[j : j + 1, :] * pad_ref[start + j : start + j + rows, :chans]
    return total * jax.nn.sigmoid(total)


def precise(a, b, contract=(1, 0)):
    return lax.dot_general(
        a,
        b,
        (((contract[0],), (contract[1],)), ((), ())),
        precision=highest,
        preferred_element_type=f32,
    )


def spread(heads, chans):
    head = lax.broadcasted_iota(jnp.int32, (heads, chans), 0)
    chan = lax.broadcasted_iota(jnp.int32, (heads, chans), 1)
    return (chan // (chans // heads) == head).astype(f32)


def front_body(capacity, experts, chunk_rows, *refs):
    inputs, refs = refs[:13], refs[13:]
    outputs, refs = refs[:5], refs[5:]
    held_in, refs = refs[:13], refs[13:]
    held_out, refs = refs[:5], refs[5:]
    scr, pad_ref, values_ref, in_sems, out_sems = refs
    arriving = [
        pltpu.make_async_copy(source, target, in_sems.at[i])
        for i, (source, target) in enumerate(zip(inputs, held_in))
    ]
    leaving = [
        pltpu.make_async_copy(source, target, out_sems.at[i])
        for i, (source, target) in enumerate(zip(held_out, outputs))
    ]
    for copy in arriving:
        copy.start()
    x_ref, gain_ref, routes_ref, heads_ref, write_ref, read_ref, tail_ref = held_in[:7]
    pre_ref, extra_ref, rate_ref, head_taps, write_taps, read_taps = held_in[7:]
    normed_ref, out_ref, local_ref, read_out, grow_out = held_out
    for copy in arriving[:3]:
        copy.wait()
    place_rows(capacity, experts, chunk_rows, x_ref, gain_ref, routes_ref, normed_ref, scr)
    leaving[0].start()
    for copy in arriving[3:]:
        copy.wait()
    rows, chans = heads_ref.shape
    heads = pre_ref.shape[0]
    tail = tail_ref[...]
    values_ref[...] = conv_silu(heads_ref, tail[:, :chans], head_taps, pad_ref)
    write = conv_silu(write_ref, tail[:, chans : chans + STATE], write_taps, pad_ref)
    read = conv_silu(read_ref, tail[:, chans + STATE :], read_taps, pad_ref)
    read_out[...] = read
    pre = pre_ref[...]
    step = jnp.maximum(pre, 0.0) + jnp.log1p(jnp.exp(-jnp.abs(pre)))
    heads_across = lax.broadcasted_iota(jnp.int32, (heads, heads), 1)
    heads_down = lax.broadcasted_iota(jnp.int32, (heads, heads), 0)
    rate = jnp.sum(
        jnp.where(heads_across == heads_down, jnp.exp(rate_ref[...]), 0.0), axis=1, keepdims=True
    )
    log_rate = -rate * step + extra_ref[...]
    row = lax.broadcasted_iota(jnp.int32, (rows, rows), 0)
    col = lax.broadcasted_iota(jnp.int32, (rows, rows), 1)
    lower = row >= col
    cum = precise(log_rate, (row <= col).astype(f32))
    cum_down = precise(lower.astype(f32), log_rate, (1, 1))
    step_down = precise((row == col).astype(f32), step, (1, 1))
    grow_out[...] = jnp.exp(cum_down)
    wide = spread(heads, chans)
    to_end = step_down * jnp.exp(cum_down[rows - 1 : rows, :] - cum_down)
    ending = values_ref[...] * precise(to_end, wide)
    state = precise(ending, write, (0, 0))
    chunks = experts
    base = chunk_rows - 24
    repeat = chunks // heads
    chunk = lax.broadcasted_iota(jnp.int32, (chunks, heads), 0)
    head = lax.broadcasted_iota(jnp.int32, (chunks, heads), 1)
    total = precise((chunk // repeat == head).astype(f32), cum)[:, rows - 1 : rows]
    top = total.astype(bf16).astype(f32)
    middle = (total - top).astype(bf16).astype(f32)
    bottom = total - top - middle
    lane = lax.broadcasted_iota(jnp.int32, (chunks, STATE), 1)
    decays = jnp.where(
        lane == 0, top, jnp.where(lane == 1, middle, jnp.where(lane == 2, bottom, 0.0))
    )
    for j in range(chunks):
        row = chunk_rows * j + base
        scr[row : row + 16, :] = state[16 * j : 16 * j + 16, :]
        scr[row + 16 : row + 24, :] = jnp.broadcast_to(decays[j : j + 1, :], (8, STATE))
    out_ref[...] = scr[...].astype(bf16)
    leaving[1].start()
    affinity = precise(read, write, (1, 1))
    left = lax.broadcasted_iota(jnp.int32, (rows, LANE), 1) < HEAD_DIM
    for pair in range(heads // 2):
        mixed = []
        for e in (2 * pair, 2 * pair + 1):
            gap = cum_down[:, e : e + 1] - cum[e : e + 1, :]
            within = jnp.exp(jnp.where(lower, gap, -jnp.inf))
            mixed.append(affinity * within * step[e : e + 1, :])
        cols = slice(pair * LANE, (pair + 1) * LANE)
        part = precise(jnp.concatenate(mixed, axis=0), values_ref[:, cols])
        local_ref[:, cols] = jnp.where(left, part[:rows], part[rows:])
    for copy in leaving[2:]:
        copy.start()
    for copy in leaving:
        copy.wait()


def carry_body(in_ref, out_ref, scr, sums):
    chunks = in_ref.shape[0]
    scr[...] = in_ref[...].astype(f32).reshape(scr.shape)
    lane = lax.broadcasted_iota(jnp.int32, (chunks, STATE), 1)
    pieces = scr[pl.ds(16, chunks, stride=24), :]
    decay = jnp.sum(jnp.where(lane < 3, pieces, 0.0), axis=1, keepdims=True)
    row = lax.broadcasted_iota(jnp.int32, (chunks, chunks), 0)
    col = lax.broadcasted_iota(jnp.int32, (chunks, chunks), 1)
    held = jnp.broadcast_to(decay, (chunks, STATE))
    ends = precise((row >= col).astype(f32), held)[:, :chunks]
    ends_across = precise(held, (row <= col).astype(f32), (0, 0))[0:1, :]
    carry = jnp.exp(jnp.where(row > col, ends - decay - ends_across, -jnp.inf))
    for r in range(0, 16, 2):
        both = jnp.concatenate(
            [
                scr[pl.ds(r, chunks, stride=24), :],
                scr[pl.ds(r + 1, chunks, stride=24), :],
            ],
            axis=1,
        )
        part = precise(carry, both)
        sums[pl.ds(r, chunks, stride=16), :] = part[:, :STATE]
        sums[pl.ds(r + 1, chunks, stride=16), :] = part[:, STATE:]
    out_ref[...] = sums[...].astype(bf16)


def mixer_out_body(
    place_ref, state_ref, read_ref, grow_ref, local_ref, gate_ref, gain_ref, weight_ref, *refs
):
    outs = refs[:-2]
    normed_ref, total_ref = refs[-2:]
    rows, chans = local_ref.shape
    heads = grow_ref.shape[1]
    carried = precise(read_ref[...], state_ref[...].astype(f32), (1, 1))
    scan_out = local_ref[...] + carried * precise(grow_ref[...], spread(heads, chans))
    gate = gate_ref[...].astype(f32)
    gated = scan_out * (gate * jax.nn.sigmoid(gate))
    gated = gated * lax.rsqrt(jnp.mean(gated * gated, axis=-1, keepdims=True) + eps_norm)
    normed_ref[...] = (gated * gain_ref[...]).astype(bf16)
    total_ref[...] = jnp.dot(normed_ref[...], weight_ref[...], preferred_element_type=f32)
    parts = len(outs)
    block = rows // parts
    for by, out in enumerate(outs):
        target = lax.rem(place_ref[0] + by, parts)
        out[...] = total_ref[pl.ds(pl.multiple_of(target * block, block), block), :].astype(bf16)


def layer(
    head_inputs_unfiltered,
    group_write_vectors,
    group_read_vectors,
    output_gate_inputs,
    step_preactivation,
    extra_decay_logs,
    head_decay_logs,
    head_filter_taps,
    write_filter_taps,
    read_filter_taps,
    grouped_norm_gain,
    mixer_output_weight,
    expert_input_rows,
    expert_norm_gain,
    routes,
    router_chosen_scores,
    routed_gate_weight,
    routed_up_weight,
    routed_down_weight,
    shared_gate_weight,
    shared_up_weight,
    shared_down_weight,
):
    tp_count = lax.axis_size("tp")
    tp_index = lax.axis_index("tp")
    ep_count = lax.axis_size(EP)
    core = lax.axis_index("ep_2")
    rows, width = expert_input_rows.shape
    experts = routed_gate_weight.shape[0] * ep_count
    capacity = 3 * rows * routes.shape[1] // (2 * experts)
    slots = experts * capacity
    pieces = width // LANE
    exchanged = (experts, capacity * pieces, LANE)

    mix_rows, head_chans = head_inputs_unfiltered.shape
    taps = head_filter_taps.shape[0]
    tail_rows = jnp.concatenate(
        [
            head_inputs_unfiltered[mix_rows - taps + 1 :],
            group_write_vectors[mix_rows - taps + 1 :],
            group_read_vectors[mix_rows - taps + 1 :],
        ],
        axis=1,
    )
    tail_rows = shift(tail_rows, EP, 1, False)
    gate, up, down = routed_gate_weight[0], routed_up_weight[0], routed_down_weight[0]
    low_gate = shift(gate, "tp", 1, True)
    high_gate = shift(gate, "tp", -1, True)
    low_up = shift(up, "tp", 1, True)
    high_up = shift(up, "tp", -1, True)

    heads = step_preactivation.shape[0]
    chunk_rows = capacity * pieces + 24
    front_in = (
        expert_input_rows,
        expert_norm_gain[None, :],
        routes.T,
        head_inputs_unfiltered,
        group_write_vectors,
        group_read_vectors,
        tail_rows,
        step_preactivation,
        extra_decay_logs,
        head_decay_logs[None, :],
        head_filter_taps,
        write_filter_taps,
        read_filter_taps,
    )
    front_out = (
        jax.ShapeDtypeStruct((rows, width), bf16),
        jax.ShapeDtypeStruct((experts * chunk_rows, LANE), bf16),
        jax.ShapeDtypeStruct((mix_rows, head_chans), f32),
        jax.ShapeDtypeStruct((mix_rows, STATE), f32),
        jax.ShapeDtypeStruct((mix_rows, heads), f32),
    )
    in_hbm = pl.BlockSpec(memory_space=pltpu.HBM)
    normed, sent, local_part, read_values, growth = pl.pallas_call(
        functools.partial(front_body, capacity, experts, chunk_rows),
        out_shape=front_out,
        in_specs=[in_hbm] * len(front_in),
        out_specs=(in_hbm,) * len(front_out),
        scratch_shapes=[pltpu.VMEM(v.shape, v.dtype) for v in front_in + front_out]
        + [
            pltpu.VMEM((experts * chunk_rows, LANE), f32),
            pltpu.VMEM((mix_rows + 8, head_chans), f32),
            pltpu.VMEM((mix_rows, head_chans), f32),
            pltpu.SemaphoreType.DMA((len(front_in),)),
            pltpu.SemaphoreType.DMA((len(front_out),)),
        ],
        compiler_params=pltpu.CompilerParams(vmem_limit_bytes=60 * MIB),
        name="front",
    )(*front_in)
    arrived = lax.all_to_all(
        sent.reshape(experts, chunk_rows, LANE), EP, 0, 0, tiled=True
    )
    half = down.shape[0] // 2
    down_a, down_b = down[:half], down[half:]
    low_down_a = shift(down_a, "tp", 1, True)
    high_down_b = shift(down_b, "tp", -1, True)
    low_down_b = shift(down_b, "tp", 1, True)
    high_down_a = shift(down_a, "tp", -1, True)
    partner = shift(normed, "ep_2", 1, True)
    far_gate = shift(low_gate, "tp", 1, True)
    far_up = shift(high_up, "tp", -1, True)
    far_down_a = shift(low_down_a, "tp", 1, True)
    far_down_b = shift(high_down_b, "tp", -1, True)
    entering = pl.pallas_call(
        carry_body,
        out_shape=jax.ShapeDtypeStruct((ep_count * 16, STATE), bf16),
        grid=(1,),
        in_specs=[
            pl.BlockSpec((ep_count, 24, STATE), lambda i: (0, capacity * pieces // 24, 0))
        ],
        out_specs=pl.BlockSpec((ep_count * 16, STATE), lambda i: (0, 0)),
        scratch_shapes=[
            pltpu.VMEM((ep_count * 24, STATE), f32),
            pltpu.VMEM((ep_count * 16, STATE), f32),
        ],
        compiler_params=pltpu.CompilerParams(vmem_limit_bytes=8 * MIB),
        name="carry",
    )(arrived)
    entering = lax.all_to_all(entering.reshape(ep_count, 16, STATE), EP, 0, 0, tiled=True)

    expert_rows, expert_sum = call(
        functools.partial(expert_first_body, capacity, chunk_rows),
        (
            jax.ShapeDtypeStruct((slots, width), bf16),
            jax.ShapeDtypeStruct((slots, width), f32),
        ),
        [pltpu.VMEM((experts * chunk_rows, LANE), f32)],
        50,
    )(
        arrived.reshape(experts * chunk_rows, LANE),
        gate,
        up,
        down,
        low_gate,
        low_up,
        low_down_a,
        low_down_b,
        high_gate,
        high_up,
        high_down_a,
        high_down_b,
    )
    far_hidden = call(
        expert_hidden_body, jax.ShapeDtypeStruct((slots, down.shape[0]), bf16), (), 16
    )(expert_rows, far_gate, far_up)
    sent_back = call(
        functools.partial(expert_last_body, capacity),
        jax.ShapeDtypeStruct((slots * pieces, LANE), bf16),
        [pltpu.VMEM((slots * pieces, LANE), f32)],
        24,
    )(far_hidden, expert_sum, far_down_a, far_down_b)
    returned = lax.all_to_all(sent_back.reshape(exchanged), EP, 0, 0, tiled=True)

    block = mix_rows // tp_count
    mix_parts = pl.pallas_call(
        mixer_out_body,
        out_shape=[jax.ShapeDtypeStruct((block, width), bf16)] * tp_count,
        in_specs=[pl.BlockSpec(memory_space=pltpu.SMEM)]
        + [pl.BlockSpec(memory_space=pltpu.VMEM)] * 7,
        scratch_shapes=[
            pltpu.VMEM((mix_rows, head_chans), bf16),
            pltpu.VMEM((mix_rows, width), f32),
        ],
        compiler_params=pltpu.CompilerParams(vmem_limit_bytes=20 * MIB),
        name="mixer_out",
    )(
        tp_index[None].astype(jnp.int32),
        entering.reshape(ep_count * 16, STATE),
        read_values,
        growth,
        local_part,
        output_gate_inputs,
        grouped_norm_gain[None, :],
        mixer_output_weight,
    )
    mix_parts = [shift(part, "tp", by, True) if by else part for by, part in enumerate(mix_parts)]
    mixer_result = sum(part.astype(f32) for part in mix_parts).astype(bf16)

    units = shared_down_weight.shape[0] // 2
    shared_own = pl.pallas_call(
        shared_pack_body,
        out_shape=jax.ShapeDtypeStruct((width + pieces * units, LANE), bf16),
        in_specs=[pl.BlockSpec(memory_space=pltpu.SMEM)]
        + [pl.BlockSpec(memory_space=pltpu.VMEM)] * 3,
        compiler_params=pltpu.CompilerParams(vmem_limit_bytes=8 * MIB),
        name="shared_pack",
    )(
        core[None].astype(jnp.int32),
        shared_gate_weight,
        shared_up_weight,
        shared_down_weight,
    )
    shared_low = shift(shared_own, "tp", 1, True)
    shared_high = shift(shared_own, "tp", -1, True)
    shared_far = shift(shared_low, "tp", 1, True)
    shared_sum, shared_send = call(
        shared_body,
        (
            jax.ShapeDtypeStruct((rows, width), f32),
            jax.ShapeDtypeStruct((rows, width), bf16),
        ),
        (),
        16,
    )(normed, partner, shared_own, shared_low, shared_high, shared_far)
    shared_got = shift(shared_send, "ep_2", 1, True)

    moe_result = call(
        functools.partial(combine_body, capacity, experts),
        jax.ShapeDtypeStruct((rows, width), bf16),
        [pltpu.VMEM((slots * pieces, LANE), f32)],
        16,
    )(
        returned.reshape(slots * pieces, LANE),
        routes,
        router_chosen_scores,
        shared_sum,
        shared_got,
    )
    return (mixer_result, moe_result)


def solution(mesh):
    split = Mesh(mesh.devices.reshape(8, 4, 2, mesh.shape["tp"]), ("ep_0", "ep_1", "ep_2", "tp"))
    placed = (
        P(EP, "tp"),
        P(EP, "tp"),
        P(EP, "tp"),
        P(EP, "tp"),
        P("tp", EP),
        P("tp", EP),
        P("tp"),
        P(None, "tp"),
        P(None, "tp"),
        P(None, "tp"),
        P("tp"),
        P("tp", None),
        P(EP_TP, None),
        P(),
        P(EP_TP, None),
        P(EP_TP, None),
        P(EP, None, "tp"),
        P(EP, None, "tp"),
        P(EP, "tp", None),
        P(None, "tp"),
        P(None, "tp"),
        P("tp", None),
    )
    return jax.shard_map(
        layer,
        mesh=split,
        in_specs=placed,
        out_specs=(P(EP_TP, None), P(EP_TP, None)),
        check_vma=False,
    )
```

time: 205 us -> 244 us (1.19)
  waiting for transfers between devices: 83 us -> 127 us
  Pallas kernels: 22.7 us -> 36.2 us
  other arithmetic: 10.8 us -> 1.77 us
  local copies, waits for them, and re-layouts: 26.6 us -> 17.9 us
  matrix products: 5.99 us -> 0 us
  starting transfers between devices: 53.6 us -> 58.6 us
    ppermute x16 -> x21, waiting for transfers between devices: 63.5 us -> 127 us  [shift(): return lax.ppermute(value, axis, pairs)]
    all_to_all x4 -> x3, waiting for transfers between devices: 19.4 us -> 0.01 us  [the longest x1 0.01 us: layer(): lax.all_to_all(sent.reshape(experts, chunk_rows, LANE), EP, 0, 0, tiled=T...]
    pallas_call x4 -> x8, Pallas kernels: 20 us -> 33.6 us  [the longest x1 10.4 us: layer(): call(functools.partial(expert_first_body, capacity, chunk_rows), (jax.Sha...]
    ppermute x16 -> x21, starting transfers between devices: 15.8 us -> 24.9 us  [shift(): return lax.ppermute(value, axis, pairs)]
    slice x14 -> x4, local copies, waits for them, and re-layouts: 10.7 us -> 2.2 us  [the longest x1 0.72 us: layer(): head_inputs_unfiltered[mix_rows - taps + 1:]]
    dot_general x8 -> x0, matrix products: 5.99 us -> none  [the longest x1 2.18 us: mixer_rows(): jnp.einsum('gels,sgep->lgep', affinity[:, None] * within, weighted, preci...]
    all_to_all x4 -> x3, starting transfers between devices: 37.8 us -> 33.8 us  [the longest x1 13 us: layer(): lax.all_to_all(sent.reshape(experts, chunk_rows, LANE), EP, 0, 0, tiled=T...]
    concatenate x4 -> x1, other arithmetic: 3.67 us -> 0.01 us  [layer(): jnp.concatenate([head_inputs_unfiltered[mix_rows - taps + 1:], group_writ...]
  transfers between devices with their start and end apart: 20 -> 24, of which waited for: 8 -> 7; matrix products, arithmetic and copies ran while one was open for 17% -> 1% of each run, Pallas kernels for 10% -> 11%
where the time goes in v1:
time: 244 us; the launch traced here: 242 us
  waiting for transfers between devices  127 us (52%)
  starting transfers between devices  58.6 us (24%)
  Pallas kernels  36.2 us (15%)
  local copies, waits for them, and re-layouts  17.9 us (7%)
    ppermute x21, waiting for transfers between devices, shift(): return lax.ppermute(value, axis, pairs)  127 us
    ppermute x21, starting transfers between devices, shift(): return lax.ppermute(value, axis, pairs)  24.9 us
    unnamed x52, local copies, waits for them, and re-layouts  15.7 us
    all_to_all x1, starting transfers between devices, layer(): lax.all_to_all(sent.reshape(experts, chunk_rows, LANE), EP, 0, 0, tiled=T...  13 us
    all_to_all x1, starting transfers between devices, layer(): lax.all_to_all(sent_back.reshape(exchanged), EP, 0, 0, tiled=True)  10.4 us
    pallas_call x1, Pallas kernels, layer(): call(functools.partial(expert_first_body, capacity, chunk_rows), (jax.Sha...  10.4 us
    all_to_all x1, starting transfers between devices, layer(): lax.all_to_all(entering.reshape(ep_count, 16, STATE), EP, 0, 0, tiled=True)  10.3 us
    pallas_call x1, Pallas kernels, layer(): pl.pallas_call(functools.partial(front_body, capacity, experts, chunk_row...  6.6 us
  transfers between devices with their start and end apart: 24, of which 7 were waited for; matrix products, arithmetic and copies ran while one was open for 1% of the time, Pallas kernels for 11%

profile of v1, /device:TPU:2, one launch (start us, length us, event | category | flops | bytes accessed | tf_op | source)
XLA Modules:
  0.0 242.0 jit_solution(557939130877225996)
XLA Ops:
  0.6 0.7 slice.23
  1.3 0.7 slice.22
  2.0 0.7 slice.21
  2.7 1.9 collective-permute-start
  4.7 3.1 %collective-permute-done.refs_6_ = bf16[3,1280]{1,0:T(4,128)(2,1)S(1)} collective-permute-done((bf16[3,1280]{1,0:T(4,128)(2,1)S(1)}, bf16[3,1280]{1,0:T(4,128)(2,1)S(1)}, u32[]{:S(2)}, u32[]{:S(2)}) %collective-permute-start) | collective-permute-done | bytes 7712 | tf_op jit(solution)/shard_map/ppermute | solution.py:34
  7.7 0.6 copy-done.22
  8.3 6.6 %front.1 = (bf16[128,2048]{1,0:T(8,128)(2,1)}, bf16[7680,128]{1,0:T(8,128)(2,1)}, f32[128,1024]{1,0:T(8,128)}, f32[128,128]{1,0:T(8,128)}, f32[128,16]{1,0:T(8,128)}) custom-call(bf16[128,2048]{1,0:T(8,128)(2,1)} %refs_0_.1, f32[1,2048]{1,0:T(1,128)} %bitcast.28, s32[2,128]{1,0:T(2,128)} %bitcast.29, bf16[128,1024]{1,0:T(8,128)(2,1)} %refs_3_.1, ...), custom_call_target="tpu_custom_call" | custom-call | tf_op jit(solution)/shard_map/front/pallas_call | solution.py:466
  14.9 13.0 %all-to-all-start = ((bf16[64,120,128]{2,1,0:T(8,128)(2,1)}), bf16[64,120,128]{2,1,0:T(8,128)(2,1)S(1)}, u32[]{:S(2)}, u32[]{:S(2)}) async-start(bf16[64,120,128]{2,1,0:T(8,128)(2,1)} %bitcast.24), calls=%async_computation | async-start | bytes 3932160 | tf_op jit(solution)/shard_map/all_to_all | solution.py:482
  28.0 1.7 collective-permute-start.4
  29.6 1.7 collective-permute-start.9
  31.4 0.4 collective-permute-start.6
  31.9 1.6 collective-permute-start.7
  33.4 1.7 collective-permute-start.10
  35.1 31.7 %collective-permute-done.6.d1a = bf16[128,2048]{1,0:T(8,128)(2,1)S(1)} collective-permute-done((bf16[128,2048]{1,0:T(8,128)(2,1)S(1)}, bf16[128,2048]{1,0:T(8,128)(2,1)S(1)}, u32[]{:S(2)}, u32[]{:S(2)}) %collective-permute-start.6) | collective-permute-done | bytes 524320 | tf_op jit(solution)/shard_map/ppermute | solution.py:34
  67.1 10.9 %collective-permute-done.7.d1b = bf16[128,2048]{1,0:T(8,128)(2,1)S(1)} collective-permute-done((bf16[128,2048]{1,0:T(8,128)(2,1)S(1)}, bf16[128,2048]{1,0:T(8,128)(2,1)S(1)}, u32[]{:S(2)}, u32[]{:S(2)}) %collective-permute-start.7) | collective-permute-done | bytes 524320 | tf_op jit(solution)/shard_map/ppermute | solution.py:34
  78.0 1.8 collective-permute-start.8
  80.0 3.0 %collective-permute-start.13 = (bf16[2048,256]{1,0:T(8,128)(2,1)}, bf16[2048,256]{1,0:T(8,128)(2,1)}, u32[]{:S(2)}, u32[]{:S(2)}) collective-permute-start(bf16[2048,256]{1,0:T(8,128)(2,1)} %collective-permute-done.9.u2), channel_id=1, source_target_pairs={{0,3},{1,0},{2,1},{3,2},{4,7},{5,4},{6,5},{7,6},{8,11},{9,8},{10,9... | collective-permute-start | bytes 3145736 | tf_op jit(solution)/shard_map/ppermute | solution.py:34
  83.0 0.8 copy-done.12
  83.8 51.8 %collective-permute-done.11.d2b = bf16[128,2048]{1,0:T(8,128)(2,1)} collective-permute-done((bf16[128,2048]{1,0:T(8,128)(2,1)S(1)}, bf16[128,2048]{1,0:T(8,128)(2,1)}, u32[]{:S(2)}, u32[]{:S(2)}) %collective-permute-start.11) | collective-permute-done | bytes 524320 | tf_op jit(solution)/shard_map/ppermute | solution.py:34
  135.9 1.0 copy-done.21
  136.9 3.0 %collective-permute-start.15 = (bf16[128,2048]{1,0:T(8,128)(2,1)}, bf16[128,2048]{1,0:T(8,128)(2,1)}, u32[]{:S(2)}, u32[]{:S(2)}) collective-permute-start(bf16[128,2048]{1,0:T(8,128)(2,1)} %collective-permute-done.11.d2b), channel_id=1, source_target_pairs={{0,3},{1,0},{2,1},{3,2},{4,7},{5,4},{6,5},{7,6},{8,11},{9,8},{10,9... | collective-permute-start | bytes 1572872 | tf_op jit(solution)/shard_map/ppermute | solution.py:34
  139.9 1.8 carry.1
  141.7 10.3 %all-to-all-start.1 = ((bf16[64,16,128]{2,1,0:T(8,128)(2,1)}), bf16[64,16,128]{2,1,0:T(8,128)(2,1)S(1)}, u32[]{:S(2)}, u32[]{:S(2)}) async-start(bf16[64,16,128]{2,1,0:T(8,128)(2,1)} %bitcast.5), calls=%async_computation.1 | async-start | bytes 524288 | tf_op jit(solution)/shard_map/all_to_all | solution.py:511
  152.0 1.0 copy-done.11
  153.1 1.0 copy-done.13
  154.1 10.4 %shard_map.221 = (bf16[384,2048]{1,0:T(8,128)(2,1)}, f32[384,2048]{1,0:T(8,128)}) custom-call(bf16[7680,128]{1,0:T(8,128)(2,1)} %bitcast.19, bf16[2048,256]{1,0:T(8,128)(2,1)} %bitcast.9.g0, bf16[2048,256]{1,0:T(8,128)(2,1)} %bitcast.26, bf16[256,2048]{1,0:T(8,128)(2,1)} %bitcast.23, bf16[2048,256]{1,0:T(8,128)(2,1)} %collective-permute-done.4.g1, ...), custom_call_target="tpu_custom_call" | custom-call | tf_op jit(solution)/shard_map/pallas_call | solution.py:513
  164.5 1.5 copy-done.3
  166.1 2.5 %shard_map.222.hidden_ref = bf16[384,256]{1,0:T(8,128)(2,1)S(1)} custom-call(bf16[384,2048]{1,0:T(8,128)(2,1)S(1)} %copy-done.3, bf16[2048,256]{1,0:T(8,128)(2,1)} %collective-permute-done.12.g, bf16[2048,256]{1,0:T(8,128)(2,1)} %collective-permute-done.13.u), custom_call_target="tpu_custom_call" | custom-call | tf_op jit(solution)/shard_map/pallas_call | solution.py:535
  168.6 5.1 %shard_map.223 = bf16[6144,128]{1,0:T(8,128)(2,1)} custom-call(bf16[384,256]{1,0:T(8,128)(2,1)S(1)} %shard_map.222.hidden_ref, f32[384,2048]{1,0:T(8,128)S(1)} %copy-done.2, bf16[128,2048]{1,0:T(8,128)(2,1)} %collective-permute-done.14.da, bf16[128,2048]{1,0:T(8,128)(2,1)} %collective-permute-done.15.db), custom_call_target="tpu_custom_call" | custom-call | tf_op jit(solution)/shard_map/pallas_call | solution.py:538
  173.7 10.4 %all-to-all-start.2 = ((bf16[64,96,128]{2,1,0:T(8,128)(2,1)}), bf16[64,96,128]{2,1,0:T(8,128)(2,1)S(1)}, u32[]{:S(2)}, u32[]{:S(2)}) async-start(bf16[64,96,128]{2,1,0:T(8,128)(2,1)} %bitcast.14), calls=%async_computation.2 | async-start | bytes 3145728 | tf_op jit(solution)/shard_map/all_to_all | solution.py:544
  184.2 1.0 copy-done.7
  185.2 1.0 copy-done.8
  186.3 0.5 shared_pack.1.own
  187.1 3.2 %collective-permute-start.18 = (bf16[3072,128]{1,0:T(8,128)(2,1)S(1)}, bf16[3072,128]{1,0:T(8,128)(2,1)}, u32[]{:S(2)}, u32[]{:S(2)}) collective-permute-start(bf16[3072,128]{1,0:T(8,128)(2,1)S(1)} %shared_pack.1.own), channel_id=1, source_target_pairs={{0,3},{1,0},{2,1},{3,2},{4,7},{5,4},{6,5},{7,6},{8,11},{9,8},{10,9... | collective-permute-start | bytes 2359304 | tf_op jit(solution)/shard_map/ppermute | solution.py:34
  190.3 17.5 %collective-permute-done.17.low = bf16[3072,128]{1,0:T(8,128)(2,1)S(1)} collective-permute-done((bf16[3072,128]{1,0:T(8,128)(2,1)S(1)}, bf16[3072,128]{1,0:T(8,128)(2,1)S(1)}, u32[]{:S(2)}, u32[]{:S(2)}) %collective-permute-start.17) | collective-permute-done | bytes 786464 | tf_op jit(solution)/shard_map/ppermute | solution.py:34
  207.9 2.5 %copy-done.1 = bf16[1024,2048]{1,0:T(8,128)(2,1)S(1)} copy-done((bf16[1024,2048]{1,0:T(8,128)(2,1)S(1)}, bf16[1024,2048]{1,0:T(8,128)(2,1)}, u32[]{:S(2)}) %copy-start.1) | copy-done | bytes 4194328
  210.3 1.0 copy-done.9
  211.4 0.9 copy-done.15
  212.3 0.8 copy-done.16
  213.2 0.8 copy-done.17
  214.0 2.7 %mixer_out.1 = (bf16[32,2048]{1,0:T(8,128)(2,1)S(1)}, bf16[32,2048]{1,0:T(8,128)(2,1)}, bf16[32,2048]{1,0:T(8,128)(2,1)}, bf16[32,2048]{1,0:T(8,128)(2,1)}) custom-call(s32[1]{0:T(128)} %bitcast.place_ref, bf16[1024,128]{1,0:T(8,128)(2,1)S(1)} %bitcast.21, f32[128,128]{1,0:T(8,128)S(1)} %copy-done.16, f32[128,16]{1,0:T(8,128)S(1)} %copy-done.17, ...), custom_call_target="tpu_custom_call" | custom-call | tf_op jit(solution)/shard_map/mixer_out/pallas_call | solution.py:547
  216.7 2.9 %collective-permute-start.3 = (bf16[32,2048]{1,0:T(8,128)(2,1)}, bf16[32,2048]{1,0:T(8,128)(2,1)}, u32[]{:S(2)}, u32[]{:S(2)}) collective-permute-start(bf16[32,2048]{1,0:T(8,128)(2,1)} %get-tuple-element.22), channel_id=1, source_target_pairs={{0,3},{1,0},{2,1},{3,2},{4,7},{5,4},{6,5},{7,6},{8,11},{9,8},{10,9... | collective-permute-start | bytes 393224 | tf_op jit(solution)/shard_map/ppermute | solution.py:34
  219.7 0.8 collective-permute-start.1
  220.5 11.6 %collective-permute-done.19.far = bf16[3072,128]{1,0:T(8,128)(2,1)} collective-permute-done((bf16[3072,128]{1,0:T(8,128)(2,1)S(1)}, bf16[3072,128]{1,0:T(8,128)(2,1)}, u32[]{:S(2)}, u32[]{:S(2)}) %collective-permute-start.19) | collective-permute-done | bytes 786464 | tf_op jit(solution)/shard_map/ppermute | solution.py:34
  232.1 1.1 copy-done.5
  233.2 4.1 %shard_map.224 = (f32[128,2048]{1,0:T(8,128)S(1)}, bf16[128,2048]{1,0:T(8,128)(2,1)}) custom-call(bf16[128,2048]{1,0:T(8,128)(2,1)S(1)} %copy-done.14, bf16[128,2048]{1,0:T(8,128)(2,1)} %collective-permute-done.16.other_ref, bf16[3072,128]{1,0:T(8,128)(2,1)S(1)} %shared_pack.1.own, bf16[3072,128]{1,0:T(8,128)(2,1)S(1)} %copy-done.5, ...), custom_call_target="tpu_custom_call" | custom-call | tf_op jit(solution)/shard_map/pallas_call | solution.py:588
  237.6 1.8 add_convert_fusion
  239.4 2.6 %shard_map.225 = bf16[128,2048]{1,0:T(8,128)(2,1)} custom-call(bf16[6144,128]{1,0:T(8,128)(2,1)S(1)} %bitcast.20, s32[128,2]{1,0:T(8,128)S(1)} %copy.24.routes_ref, bf16[128,2]{1,0:T(8,128)(2,1)S(1)} %copy.25.scores_ref, f32[128,2048]{1,0:T(8,128)S(1)} %get-tuple-element.26.shared_ref, bf16[128,2048]{1,0:T(8,128)(2,1)S(1)} %collective-permute-done.20.other_ref), custom_call_target="tpu_custom_call" | custom-call | tf_op jit(solution)/shard_map/pallas_call | solution.py:599
  (67 shorter events, 1.7 us)
Async XLA Ops:
  2.7 5.0 %collective-permute-start = (bf16[3,1280]{1,0:T(4,128)(2,1)S(1)}, bf16[3,1280]{1,0:T(4,128)(2,1)S(1)}, u32[]{:S(2)}, u32[]{:S(2)}) collective-permute-start(bf16[3,1280]{1,0:T(4,128)(2,1)S(1)} %pad_maximum_fusion), channel_id=1, source_target_pairs={{0,4},{4,8},{8,12},{12,16},{16,20},{20,24},{24,28},{28,32},{32,36}... | collective-permute-start | bytes 23048 | tf_op jit(solution)/shard_map/ppermute | solution.py:34
  14.9 16.4 %copy-start.19 = (bf16[1,256,2048]{2,1,0:T(8,128)(2,1)S(1)}, bf16[1,256,2048]{2,1,0:T(8,128)(2,1)}, u32[]{:S(2)}) copy-start(bf16[1,256,2048]{2,1,0:T(8,128)(2,1)} %param.40) | copy-start | bytes 3145732
  14.9 125.0 %all-to-all-start = ((bf16[64,120,128]{2,1,0:T(8,128)(2,1)}), bf16[64,120,128]{2,1,0:T(8,128)(2,1)S(1)}, u32[]{:S(2)}, u32[]{:S(2)}) async-start(bf16[64,120,128]{2,1,0:T(8,128)(2,1)} %bitcast.24), calls=%async_computation | async-start | bytes 3932160 | tf_op jit(solution)/shard_map/all_to_all | solution.py:482
  28.0 38.8 %copy-start.20 = (bf16[1,2048,256]{2,1,0:T(8,128)(2,1)S(1)}, bf16[1,2048,256]{2,1,0:T(8,128)(2,1)}, u32[]{:S(2)}) copy-start(bf16[1,2048,256]{2,1,0:T(8,128)(2,1)} %param.39) | copy-start | bytes 3145732
  28.0 51.8 %collective-permute-start.4 = (bf16[2048,256]{1,0:T(8,128)(2,1)}, bf16[2048,256]{1,0:T(8,128)(2,1)}, u32[]{:S(2)}, u32[]{:S(2)}) collective-permute-start(bf16[2048,256]{1,0:T(8,128)(2,1)} %bitcast.9.g0), channel_id=1, source_target_pairs={{0,1},{1,2},{2,3},{3,0},{4,5},{5,6},{6,7},{7,4},{8,9},{9,10},{10,1... | collective-permute-start | bytes 3145736 | tf_op jit(solution)/shard_map/ppermute | solution.py:34
  29.6 50.4 %collective-permute-start.9 = (bf16[2048,256]{1,0:T(8,128)(2,1)}, bf16[2048,256]{1,0:T(8,128)(2,1)}, u32[]{:S(2)}, u32[]{:S(2)}) collective-permute-start(bf16[2048,256]{1,0:T(8,128)(2,1)} %bitcast.25), channel_id=1, source_target_pairs={{0,3},{1,0},{2,1},{3,2},{4,7},{5,4},{6,5},{7,6},{8,11},{9,8},{10,9... | collective-permute-start | bytes 3145736 | tf_op jit(solution)/shard_map/ppermute | solution.py:34
  31.4 35.3 %collective-permute-start.6 = (bf16[128,2048]{1,0:T(8,128)(2,1)S(1)}, bf16[128,2048]{1,0:T(8,128)(2,1)S(1)}, u32[]{:S(2)}, u32[]{:S(2)}) collective-permute-start(bf16[128,2048]{1,0:T(8,128)(2,1)S(1)} %get-tuple-element.29), channel_id=1, source_target_pairs={{0,1},{1,2},{2,3},{3,0},{4,5},{5,6},{6,7},{7,4},{8,9},{9,10},{10,1... | collective-permute-start | bytes 1572872 | tf_op jit(solution)/shard_map/ppermute | solution.py:34
  31.9 46.1 %collective-permute-start.7 = (bf16[128,2048]{1,0:T(8,128)(2,1)S(1)}, bf16[128,2048]{1,0:T(8,128)(2,1)S(1)}, u32[]{:S(2)}, u32[]{:S(2)}) collective-permute-start(bf16[128,2048]{1,0:T(8,128)(2,1)S(1)} %get-tuple-element.28), channel_id=1, source_target_pairs={{0,1},{1,2},{2,3},{3,0},{4,5},{5,6},{6,7},{7,4},{8,9},{9,10},{10,1... | collective-permute-start | bytes 1572872 | tf_op jit(solution)/shard_map/ppermute | solution.py:34
  33.4 49.6 %collective-permute-start.10 = (bf16[128,2048]{1,0:T(8,128)(2,1)S(1)}, bf16[128,2048]{1,0:T(8,128)(2,1)S(1)}, u32[]{:S(2)}, u32[]{:S(2)}) collective-permute-start(bf16[128,2048]{1,0:T(8,128)(2,1)S(1)} %get-tuple-element.29), channel_id=1, source_target_pairs={{0,3},{1,0},{2,1},{3,2},{4,7},{5,4},{6,5},{7,6},{8,11},{9,8},{10,9... | collective-permute-start | bytes 1572872 | tf_op jit(solution)/shard_map/ppermute | solution.py:34
  66.8 69.1 %collective-permute-start.5 = (bf16[2048,256]{1,0:T(8,128)(2,1)S(1)}, bf16[2048,256]{1,0:T(8,128)(2,1)S(1)}, u32[]{:S(2)}, u32[]{:S(2)}) collective-permute-start(bf16[2048,256]{1,0:T(8,128)(2,1)S(1)} %bitcast.27), channel_id=1, source_target_pairs={{0,1},{1,2},{2,3},{3,0},{4,5},{5,6},{6,7},{7,4},{8,9},{9,10},{10,1... | collective-permute-start | bytes 3145736 | tf_op jit(solution)/shard_map/ppermute | solution.py:34
  78.0 63.7 %copy-start.10 = (bf16[128,2048]{1,0:T(8,128)(2,1)}, bf16[128,2048]{1,0:T(8,128)(2,1)S(1)}, u32[]{:S(2)}) copy-start(bf16[128,2048]{1,0:T(8,128)(2,1)S(1)} %collective-permute-done.7.d1b) | copy-start | bytes 1572868
  78.0 74.0 %collective-permute-start.8 = (bf16[2048,256]{1,0:T(8,128)(2,1)}, bf16[2048,256]{1,0:T(8,128)(2,1)}, u32[]{:S(2)}, u32[]{:S(2)}) collective-permute-start(bf16[2048,256]{1,0:T(8,128)(2,1)} %bitcast.9.g0), channel_id=1, source_target_pairs={{0,3},{1,0},{2,1},{3,2},{4,7},{5,4},{6,5},{7,6},{8,11},{9,8},{10,9... | collective-permute-start | bytes 3145736 | tf_op jit(solution)/shard_map/ppermute | solution.py:34
  79.8 84.7 %collective-permute-start.12 = (bf16[2048,256]{1,0:T(8,128)(2,1)}, bf16[2048,256]{1,0:T(8,128)(2,1)}, u32[]{:S(2)}, u32[]{:S(2)}) collective-permute-start(bf16[2048,256]{1,0:T(8,128)(2,1)} %collective-permute-done.4.g1), channel_id=1, source_target_pairs={{0,1},{1,2},{2,3},{3,0},{4,5},{5,6},{6,7},{7,4},{8,9},{9,10},{10,1... | collective-permute-start | bytes 3145736 | tf_op jit(solution)/shard_map/ppermute | solution.py:34
  80.0 84.5 %collective-permute-start.13 = (bf16[2048,256]{1,0:T(8,128)(2,1)}, bf16[2048,256]{1,0:T(8,128)(2,1)}, u32[]{:S(2)}, u32[]{:S(2)}) collective-permute-start(bf16[2048,256]{1,0:T(8,128)(2,1)} %collective-permute-done.9.u2), channel_id=1, source_target_pairs={{0,3},{1,0},{2,1},{3,2},{4,7},{5,4},{6,5},{7,6},{8,11},{9,8},{10,9... | collective-permute-start | bytes 3145736 | tf_op jit(solution)/shard_map/ppermute | solution.py:34
  83.0 0.8 copy-start.12
  83.8 51.8 %collective-permute-start.11 = (bf16[128,2048]{1,0:T(8,128)(2,1)S(1)}, bf16[128,2048]{1,0:T(8,128)(2,1)}, u32[]{:S(2)}, u32[]{:S(2)}) collective-permute-start(bf16[128,2048]{1,0:T(8,128)(2,1)S(1)} %get-tuple-element.28), channel_id=1, source_target_pairs={{0,3},{1,0},{2,1},{3,2},{4,7},{5,4},{6,5},{7,6},{8,11},{9,8},{10,9... | collective-permute-start | bytes 1572872 | tf_op jit(solution)/shard_map/ppermute | solution.py:34
  135.6 33.0 %collective-permute-start.14 = (bf16[128,2048]{1,0:T(8,128)(2,1)S(1)}, bf16[128,2048]{1,0:T(8,128)(2,1)}, u32[]{:S(2)}, u32[]{:S(2)}) collective-permute-start(bf16[128,2048]{1,0:T(8,128)(2,1)S(1)} %collective-permute-done.6.d1a), channel_id=1, source_target_pairs={{0,1},{1,2},{2,3},{3,0},{4,5},{5,6},{6,7},{7,4},{8,9},{9,10},{10,1... | collective-permute-start | bytes 1572872 | tf_op jit(solution)/shard_map/ppermute | solution.py:34
  135.9 1.0 copy-start.21
  136.9 31.7 %collective-permute-start.15 = (bf16[128,2048]{1,0:T(8,128)(2,1)}, bf16[128,2048]{1,0:T(8,128)(2,1)}, u32[]{:S(2)}, u32[]{:S(2)}) collective-permute-start(bf16[128,2048]{1,0:T(8,128)(2,1)} %collective-permute-done.11.d2b), channel_id=1, source_target_pairs={{0,3},{1,0},{2,1},{3,2},{4,7},{5,4},{6,5},{7,6},{8,11},{9,8},{10,9... | collective-permute-start | bytes 1572872 | tf_op jit(solution)/shard_map/ppermute | solution.py:34
  139.9 12.1 %copy-start = (bf16[64,120,128]{2,1,0:T(8,128)(2,1)}, bf16[64,120,128]{2,1,0:T(8,128)(2,1)S(1)}, u32[]{:S(2)}) copy-start(bf16[64,120,128]{2,1,0:T(8,128)(2,1)S(1)} %all-to-all-done.in_ref) | copy-start | bytes 5898244
  141.7 32.0 %all-to-all-start.1 = ((bf16[64,16,128]{2,1,0:T(8,128)(2,1)}), bf16[64,16,128]{2,1,0:T(8,128)(2,1)S(1)}, u32[]{:S(2)}, u32[]{:S(2)}) async-start(bf16[64,16,128]{2,1,0:T(8,128)(2,1)} %bitcast.5), calls=%async_computation.1 | async-start | bytes 524288 | tf_op jit(solution)/shard_map/all_to_all | solution.py:511
  152.0 1.0 copy-start.11
  153.1 1.0 copy-start.13
  164.5 4.1 %copy-start.2 = (f32[384,2048]{1,0:T(8,128)S(1)}, f32[384,2048]{1,0:T(8,128)}, u32[]{:S(2)}) copy-start(f32[384,2048]{1,0:T(8,128)} %get-tuple-element.24.sum_ref) | copy-start | bytes 9437188
  164.5 1.6 copy-start.3
  173.7 10.5 %copy-start.6 = (bf16[2048,128]{1,0:T(8,128)(2,1)S(1)}, bf16[2048,128]{1,0:T(8,128)(2,1)}, u32[]{:S(2)}) copy-start(bf16[2048,128]{1,0:T(8,128)(2,1)} %gate_ref.3) | copy-start | bytes 1572868
  173.7 65.7 %all-to-all-start.2 = ((bf16[64,96,128]{2,1,0:T(8,128)(2,1)}), bf16[64,96,128]{2,1,0:T(8,128)(2,1)S(1)}, u32[]{:S(2)}, u32[]{:S(2)}) async-start(bf16[64,96,128]{2,1,0:T(8,128)(2,1)} %bitcast.14), calls=%async_computation.2 | async-start | bytes 3145728 | tf_op jit(solution)/shard_map/all_to_all | solution.py:544
  184.2 23.7 %copy-start.18 = (f32[1024]{0:T(1024)S(1)}, f32[1024]{0:T(1024)}, u32[]{:S(2)}) copy-start(f32[1024]{0:T(1024)} %param.32) | copy-start | bytes 12292
  184.2 1.0 copy-start.7
  185.2 1.0 copy-start.8
  186.8 21.1 %collective-permute-start.17 = (bf16[3072,128]{1,0:T(8,128)(2,1)S(1)}, bf16[3072,128]{1,0:T(8,128)(2,1)S(1)}, u32[]{:S(2)}, u32[]{:S(2)}) collective-permute-start(bf16[3072,128]{1,0:T(8,128)(2,1)S(1)} %shared_pack.1.own), channel_id=1, source_target_pairs={{0,1},{1,2},{2,3},{3,0},{4,5},{5,6},{6,7},{7,4},{8,9},{9,10},{10,1... | collective-permute-start | bytes 2359304 | tf_op jit(solution)/shard_map/ppermute | solution.py:34
  187.1 33.4 %collective-permute-start.18 = (bf16[3072,128]{1,0:T(8,128)(2,1)S(1)}, bf16[3072,128]{1,0:T(8,128)(2,1)}, u32[]{:S(2)}, u32[]{:S(2)}) collective-permute-start(bf16[3072,128]{1,0:T(8,128)(2,1)S(1)} %shared_pack.1.own), channel_id=1, source_target_pairs={{0,3},{1,0},{2,1},{3,2},{4,7},{5,4},{6,5},{7,6},{8,11},{9,8},{10,9... | collective-permute-start | bytes 2359304 | tf_op jit(solution)/shard_map/ppermute | solution.py:34
  207.8 8.9 %copy-start.4 = (bf16[3072,128]{1,0:T(8,128)(2,1)}, bf16[3072,128]{1,0:T(8,128)(2,1)S(1)}, u32[]{:S(2)}) copy-start(bf16[3072,128]{1,0:T(8,128)(2,1)S(1)} %collective-permute-done.17.low) | copy-start | bytes 2359300
  207.8 24.2 %collective-permute-start.19 = (bf16[3072,128]{1,0:T(8,128)(2,1)S(1)}, bf16[3072,128]{1,0:T(8,128)(2,1)}, u32[]{:S(2)}, u32[]{:S(2)}) collective-permute-start(bf16[3072,128]{1,0:T(8,128)(2,1)S(1)} %collective-permute-done.17.low), channel_id=1, source_target_pairs={{0,1},{1,2},{2,3},{3,0},{4,5},{5,6},{6,7},{7,4},{8,9},{9,10},{10,1... | collective-permute-start | bytes 2359304 | tf_op jit(solution)/shard_map/ppermute | solution.py:34
  207.8 11.8 %collective-permute-start.16 = (bf16[128,2048]{1,0:T(8,128)(2,1)}, bf16[128,2048]{1,0:T(8,128)(2,1)}, u32[]{:S(2)}, u32[]{:S(2)}) collective-permute-start(bf16[128,2048]{1,0:T(8,128)(2,1)} %get-tuple-element.25.mine_ref), channel_id=1, source_target_pairs={{0,4},{4,0},{1,5},{5,1},{2,6},{6,2},{3,7},{7,3},{8,12},{12,8},{9,1... | collective-permute-start | bytes 1572872 | tf_op jit(solution)/shard_map/ppermute | solution.py:34
  207.9 2.5 %copy-start.1 = (bf16[1024,2048]{1,0:T(8,128)(2,1)S(1)}, bf16[1024,2048]{1,0:T(8,128)(2,1)}, u32[]{:S(2)}) copy-start(bf16[1024,2048]{1,0:T(8,128)(2,1)} %weight_ref.1) | copy-start | bytes 12582916
  210.3 1.0 copy-start.9
  211.4 0.9 copy-start.15
  212.3 0.8 copy-start.16
  213.2 0.8 copy-start.17
  214.0 18.1 %copy-start.14 = (bf16[128,2048]{1,0:T(8,128)(2,1)S(1)}, bf16[128,2048]{1,0:T(8,128)(2,1)}, u32[]{:S(2)}) copy-start(bf16[128,2048]{1,0:T(8,128)(2,1)} %get-tuple-element.25.mine_ref) | copy-start | bytes 1572868
  216.7 20.8 %collective-permute-start.3 = (bf16[32,2048]{1,0:T(8,128)(2,1)}, bf16[32,2048]{1,0:T(8,128)(2,1)}, u32[]{:S(2)}, u32[]{:S(2)}) collective-permute-start(bf16[32,2048]{1,0:T(8,128)(2,1)} %get-tuple-element.22), channel_id=1, source_target_pairs={{0,3},{1,0},{2,1},{3,2},{4,7},{5,4},{6,5},{7,6},{8,11},{9,8},{10,9... | collective-permute-start | bytes 393224 | tf_op jit(solution)/shard_map/ppermute | solution.py:34
  219.6 17.9 %collective-permute-start.2 = (bf16[32,2048]{1,0:T(8,128)(2,1)}, bf16[32,2048]{1,0:T(8,128)(2,1)}, u32[]{:S(2)}, u32[]{:S(2)}) collective-permute-start(bf16[32,2048]{1,0:T(8,128)(2,1)} %get-tuple-element.21), channel_id=1, source_target_pairs={{0,2},{1,3},{2,0},{3,1},{4,6},{5,7},{6,4},{7,5},{8,10},{9,11},{10,... | collective-permute-start | bytes 393224 | tf_op jit(solution)/shard_map/ppermute | solution.py:34
  219.6 17.6 %copy-start.23 = (s32[128,2]{0,1:T(2,128)S(1)}, s32[128,2]{0,1:T(2,128)}, u32[]{:S(2)}) copy-start(s32[128,2]{0,1:T(2,128)} %param.36) | copy-start | bytes 3076
  219.6 17.8 %copy-start.24 = (bf16[128,2]{0,1:T(2,128)(2,1)S(1)}, bf16[128,2]{0,1:T(2,128)(2,1)}, u32[]{:S(2)}) copy-start(bf16[128,2]{0,1:T(2,128)(2,1)} %param.37) | copy-start | bytes 1540
  219.7 17.9 %collective-permute-start.1 = (bf16[32,2048]{1,0:T(8,128)(2,1)}, bf16[32,2048]{1,0:T(8,128)(2,1)}, u32[]{:S(2)}, u32[]{:S(2)}) collective-permute-start(bf16[32,2048]{1,0:T(8,128)(2,1)} %get-tuple-element.20), channel_id=1, source_target_pairs={{0,1},{1,2},{2,3},{3,0},{4,5},{5,6},{6,7},{7,4},{8,9},{9,10},{10,1... | collective-permute-start | bytes 393224 | tf_op jit(solution)/shard_map/ppermute | solution.py:34
  232.1 1.1 copy-start.5
  237.3 2.1 collective-permute-start.20
  (1 other events, 0.6 us)

commit v2 on v1

--- a/solution.py
+++ b/solution.py
@@ -82,27 +82,26 @@
 
 
 def expert_first_body(
-    capacity, chunk_rows, in_ref, g0, u0, d0, g1, u1, d1a, d1b, g2, u2, d2a, d2b, rows_ref, sum_ref, scr
+    capacity, chunk_rows, in_ref, g0, u0, g1, u1, g2, u2, d0, d1a, d1b, d2a, d2b, rows_ref, sum_ref, scr
 ):
     slots, width = rows_ref.shape
     pieces = width // LANE
-    sources = slots // capacity
+    count = slots // capacity
     scr[...] = in_ref[...].astype(f32)
     for r in range(capacity):
         for k in range(pieces):
-            got = scr[pl.ds(r * pieces + k, sources, stride=chunk_rows), :]
-            rows_ref[r * sources : (r + 1) * sources, k * LANE : (k + 1) * LANE] = got.astype(bf16)
+            got = scr[pl.ds(r * pieces + k, count, stride=chunk_rows), :]
+            rows_ref[r * count : (r + 1) * count, k * LANE : (k + 1) * LANE] = got.astype(bf16)
     x = rows_ref[...]
     hidden = [expert_hidden(x, g[...], u[...]) for g, u in ((g0, u0), (g1, u1), (g2, u2))]
-    half = d1a.shape[0]
     for k in range(0, pieces, 2):
         cols = slice(k * LANE, (k + 2) * LANE)
+        low_down = jnp.concatenate([d1a[:, cols], d1b[:, cols]], axis=0)
+        high_down = jnp.concatenate([d2a[:, cols], d2b[:, cols]], axis=0)
         sum_ref[:, cols] = (
             jnp.dot(hidden[0], d0[:, cols], preferred_element_type=f32)
-            + jnp.dot(hidden[1][:, :half], d1a[:, cols], preferred_element_type=f32)
-            + jnp.dot(hidden[1][:, half:], d1b[:, cols], preferred_element_type=f32)
-            + jnp.dot(hidden[2][:, :half], d2a[:, cols], preferred_element_type=f32)
-            + jnp.dot(hidden[2][:, half:], d2b[:, cols], preferred_element_type=f32)
+            + jnp.dot(hidden[1], low_down, preferred_element_type=f32)
+            + jnp.dot(hidden[2], high_down, preferred_element_type=f32)
         )
 
 
@@ -114,13 +113,15 @@
     slots, width = sum_ref.shape
     pieces = width // LANE
     hidden = hidden_ref[...]
-    half = da.shape[0]
     for k in range(0, pieces, 2):
         cols = slice(k * LANE, (k + 2) * LANE)
         part = (
             sum_ref[:, cols]
-            + jnp.dot(hidden[:, :half], da[:, cols], preferred_element_type=f32)
-            + jnp.dot(hidden[:, half:], db[:, cols], preferred_element_type=f32)
+            + jnp.dot(
+                hidden,
+                jnp.concatenate([da[:, cols], db[:, cols]], axis=0),
+                preferred_element_type=f32,
+            )
         )
         sources = slots // capacity
         for r in range(capacity):
@@ -179,9 +180,7 @@
         send_ref[:, cols] = part[rows:].astype(bf16)
 
 
-def combine_body(
-    capacity, experts, in_ref, routes_ref, scores_ref, shared_ref, other_ref, out_ref, scr
-):
+def combine_body(capacity, experts, in_ref, routes_ref, scores_ref, shared_ref, out_ref, scr):
     rows, width = out_ref.shape
     pieces = width // LANE
     slots = experts * capacity
@@ -217,9 +216,7 @@
         got = jnp.dot(pick, both, preferred_element_type=f32)
         cols = slice(k * LANE, (k + 2) * LANE)
         out_ref[:, cols] = (
-            got[:rows] * w0
-            + got[rows:] * w1
-            + (shared_ref[:, cols] + other_ref[:, cols].astype(f32))
+            got[:rows] * w0 + got[rows:] * w1 + shared_ref[:, cols]
         ).astype(bf16)
 
 
@@ -244,6 +241,10 @@
         precision=highest,
         preferred_element_type=f32,
     )
+
+
+def keep_near(value):
+    return pltpu.with_memory_space_constraint(value, pltpu.VMEM)
 
 
 def spread(heads, chans):
@@ -456,11 +457,11 @@
         read_filter_taps,
     )
     front_out = (
-        jax.ShapeDtypeStruct((rows, width), bf16),
-        jax.ShapeDtypeStruct((experts * chunk_rows, LANE), bf16),
-        jax.ShapeDtypeStruct((mix_rows, head_chans), f32),
-        jax.ShapeDtypeStruct((mix_rows, STATE), f32),
-        jax.ShapeDtypeStruct((mix_rows, heads), f32),
+        pltpu.HBM((rows, width), bf16),
+        pltpu.HBM((experts * chunk_rows, LANE), bf16),
+        pltpu.HBM((mix_rows, head_chans), f32),
+        pltpu.HBM((mix_rows, STATE), f32),
+        pltpu.HBM((mix_rows, heads), f32),
     )
     in_hbm = pl.BlockSpec(memory_space=pltpu.HBM)
     normed, sent, local_part, read_values, growth = pl.pallas_call(
@@ -476,9 +477,9 @@
             pltpu.SemaphoreType.DMA((len(front_in),)),
             pltpu.SemaphoreType.DMA((len(front_out),)),
         ],
-        compiler_params=pltpu.CompilerParams(vmem_limit_bytes=60 * MIB),
+        compiler_params=pltpu.CompilerParams(vmem_limit_bytes=24 * MIB),
         name="front",
-    )(*front_in)
+    )(*(pltpu.with_memory_space_constraint(v, pltpu.HBM) for v in front_in))
     arrived = lax.all_to_all(
         sent.reshape(experts, chunk_rows, LANE), EP, 0, 0, tiled=True
     )
@@ -510,36 +511,42 @@
     )(arrived)
     entering = lax.all_to_all(entering.reshape(ep_count, 16, STATE), EP, 0, 0, tiled=True)
 
+    low_gate, low_up, low_down_a, low_down_b = map(
+        keep_near, (low_gate, low_up, low_down_a, low_down_b)
+    )
+    high_gate, high_up, high_down_a, high_down_b = map(
+        keep_near, (high_gate, high_up, high_down_a, high_down_b)
+    )
+    far_gate, far_up, far_down_a, far_down_b = map(
+        keep_near, (far_gate, far_up, far_down_a, far_down_b)
+    )
     expert_rows, expert_sum = call(
         functools.partial(expert_first_body, capacity, chunk_rows),
-        (
-            jax.ShapeDtypeStruct((slots, width), bf16),
-            jax.ShapeDtypeStruct((slots, width), f32),
-        ),
+        (pltpu.VMEM((slots, width), bf16), pltpu.VMEM((slots, width), f32)),
         [pltpu.VMEM((experts * chunk_rows, LANE), f32)],
-        50,
+        16,
     )(
         arrived.reshape(experts * chunk_rows, LANE),
         gate,
         up,
-        down,
         low_gate,
         low_up,
+        high_gate,
+        high_up,
+        down,
         low_down_a,
         low_down_b,
-        high_gate,
-        high_up,
         high_down_a,
         high_down_b,
     )
     far_hidden = call(
-        expert_hidden_body, jax.ShapeDtypeStruct((slots, down.shape[0]), bf16), (), 16
+        expert_hidden_body, jax.ShapeDtypeStruct((slots, down.shape[0]), bf16), (), 10
     )(expert_rows, far_gate, far_up)
     sent_back = call(
         functools.partial(expert_last_body, capacity),
         jax.ShapeDtypeStruct((slots * pieces, LANE), bf16),
         [pltpu.VMEM((slots * pieces, LANE), f32)],
-        24,
+        14,
     )(far_hidden, expert_sum, far_down_a, far_down_b)
     returned = lax.all_to_all(sent_back.reshape(exchanged), EP, 0, 0, tiled=True)
 
@@ -588,7 +595,7 @@
     shared_sum, shared_send = call(
         shared_body,
         (
-            jax.ShapeDtypeStruct((rows, width), f32),
+            pltpu.HBM((rows, width), f32),
             jax.ShapeDtypeStruct((rows, width), bf16),
         ),
         (),
@@ -605,8 +612,7 @@
         returned.reshape(slots * pieces, LANE),
         routes,
         router_chosen_scores,
-        shared_sum,
-        shared_got,
+        shared_sum + shared_got.astype(f32),
     )
     return (mixer_result, moe_result)
 

time: 244 us -> 248 us (1.016)
  waiting for transfers between devices: 127 us -> 142 us
  Pallas kernels: 36.2 us -> 30 us
  local copies, waits for them, and re-layouts: 17.9 us -> 14.5 us
    ppermute x21, waiting for transfers between devices: 127 us -> 142 us  [shift(): return lax.ppermute(value, axis, pairs)]
    pallas_call x2, Pallas kernels: 14.4 us -> 9.41 us  [the longest x1 6.56 us: layer(): call(functools.partial(expert_first_body, capacity, chunk_rows), (pltpu.V...]
    unnamed x52 -> x48, local copies, waits for them, and re-layouts: 15.7 us -> 12.3 us
  transfers between devices with their start and end apart: 24 -> 24, of which waited for: 7 -> 10; matrix products, arithmetic and copies ran while one was open for 1% -> 1% of each run, Pallas kernels for 11% -> 8%
where the time goes in v2:
time: 248 us; the launch traced here: 246 us
  waiting for transfers between devices  142 us (57%)
  starting transfers between devices  56.8 us (23%)
  Pallas kernels  30 us (12%)
  local copies, waits for them, and re-layouts  14.5 us (6%)
    ppermute x21, waiting for transfers between devices, shift(): return lax.ppermute(value, axis, pairs)  142 us
    ppermute x21, starting transfers between devices, shift(): return lax.ppermute(value, axis, pairs)  23.1 us
    all_to_all x1, starting transfers between devices, layer(): lax.all_to_all(sent.reshape(experts, chunk_rows, LANE), EP, 0, 0, tiled=T...  13 us
    unnamed x48, local copies, waits for them, and re-layouts  12.3 us
    all_to_all x1, starting transfers between devices, layer(): lax.all_to_all(sent_back.reshape(exchanged), EP, 0, 0, tiled=True)  10.4 us
    all_to_all x1, starting transfers between devices, layer(): lax.all_to_all(entering.reshape(ep_count, 16, STATE), EP, 0, 0, tiled=True)  10.3 us
    pallas_call x1, Pallas kernels, layer(): pl.pallas_call(functools.partial(front_body, capacity, experts, chunk_row...  6.59 us
    pallas_call x1, Pallas kernels, layer(): call(functools.partial(expert_first_body, capacity, chunk_rows), (pltpu.V...  6.56 us
  transfers between devices with their start and end apart: 24, of which 10 were waited for; matrix products, arithmetic and copies ran while one was open for 1% of the time, Pallas kernels for 8%

profile of v2, /device:TPU:2, one launch (start us, length us, event | category | flops | bytes accessed | tf_op | source)
XLA Modules:
  0.0 246.0 jit_solution(11789906791665807584)
XLA Ops:
  0.6 0.7 slice.23
  1.3 0.7 slice.22
  2.0 0.7 slice.21
  2.7 1.9 collective-permute-start
  4.7 3.1 %collective-permute-done.refs_6_ = bf16[3,1280]{1,0:T(4,128)(2,1)S(1)} collective-permute-done((bf16[3,1280]{1,0:T(4,128)(2,1)S(1)}, bf16[3,1280]{1,0:T(4,128)(2,1)S(1)}, u32[]{:S(2)}, u32[]{:S(2)}) %collective-permute-start) | collective-permute-done | bytes 7712 | tf_op jit(solution)/shard_map/ppermute | solution.py:34
  7.7 0.6 copy-done.20
  8.3 6.6 %front.1 = (bf16[128,2048]{1,0:T(8,128)(2,1)}, bf16[7680,128]{1,0:T(8,128)(2,1)}, f32[128,1024]{1,0:T(8,128)}, f32[128,128]{1,0:T(8,128)}, f32[128,16]{1,0:T(8,128)}) custom-call(bf16[128,2048]{1,0:T(8,128)(2,1)} %refs_0_.1, f32[1,2048]{1,0:T(1,128)} %bitcast.28, s32[2,128]{1,0:T(2,128)} %bitcast.29, bf16[128,1024]{1,0:T(8,128)(2,1)} %refs_3_.1, ...), custom_call_target="tpu_custom_call" | custom-call | tf_op jit(solution)/shard_map/front/pallas_call | solution.py:467
  14.9 13.0 %all-to-all-start = ((bf16[64,120,128]{2,1,0:T(8,128)(2,1)}), bf16[64,120,128]{2,1,0:T(8,128)(2,1)S(1)}, u32[]{:S(2)}, u32[]{:S(2)}) async-start(bf16[64,120,128]{2,1,0:T(8,128)(2,1)} %bitcast.27), calls=%async_computation | async-start | bytes 3932160 | tf_op jit(solution)/shard_map/all_to_all | solution.py:483
  28.0 1.7 collective-permute-start.4
  29.6 1.7 collective-permute-start.7
  31.9 1.6 collective-permute-start.9
  33.4 1.7 collective-permute-start.10
  35.1 31.8 %collective-permute-done.8.d1a = bf16[128,2048]{1,0:T(8,128)(2,1)} collective-permute-done((bf16[128,2048]{1,0:T(8,128)(2,1)S(1)}, bf16[128,2048]{1,0:T(8,128)(2,1)}, u32[]{:S(2)}, u32[]{:S(2)}) %collective-permute-start.8) | collective-permute-done | bytes 524320 | tf_op jit(solution)/shard_map/ppermute | solution.py:34
  67.2 10.8 %collective-permute-done.9.d1b = bf16[128,2048]{1,0:T(8,128)(2,1)S(1)} collective-permute-done((bf16[128,2048]{1,0:T(8,128)(2,1)S(1)}, bf16[128,2048]{1,0:T(8,128)(2,1)S(1)}, u32[]{:S(2)}, u32[]{:S(2)}) %collective-permute-start.9) | collective-permute-done | bytes 524320 | tf_op jit(solution)/shard_map/ppermute | solution.py:34
  78.0 0.8 copy-done.10
  78.8 1.8 collective-permute-start.6
  80.8 3.0 %collective-permute-start.13 = (bf16[2048,256]{1,0:T(8,128)(2,1)}, bf16[2048,256]{1,0:T(8,128)(2,1)}, u32[]{:S(2)}, u32[]{:S(2)}) collective-permute-start(bf16[2048,256]{1,0:T(8,128)(2,1)} %collective-permute-done.7.u2), channel_id=1, source_target_pairs={{0,3},{1,0},{2,1},{3,2},{4,7},{5,4},{6,5},{7,6},{8,11},{9,8},{10,9... | collective-permute-start | bytes 3145736 | tf_op jit(solution)/shard_map/ppermute | solution.py:34
  83.8 0.8 copy-done.12
  84.6 51.8 %collective-permute-done.11.d2b = bf16[128,2048]{1,0:T(8,128)(2,1)} collective-permute-done((bf16[128,2048]{1,0:T(8,128)(2,1)S(1)}, bf16[128,2048]{1,0:T(8,128)(2,1)}, u32[]{:S(2)}, u32[]{:S(2)}) %collective-permute-start.11) | collective-permute-done | bytes 524320 | tf_op jit(solution)/shard_map/ppermute | solution.py:34
  136.7 1.0 copy-done.4
  137.7 3.0 %collective-permute-start.15 = (bf16[128,2048]{1,0:T(8,128)(2,1)}, bf16[128,2048]{1,0:T(8,128)(2,1)}, u32[]{:S(2)}, u32[]{:S(2)}) collective-permute-start(bf16[128,2048]{1,0:T(8,128)(2,1)} %collective-permute-done.11.d2b), channel_id=1, source_target_pairs={{0,3},{1,0},{2,1},{3,2},{4,7},{5,4},{6,5},{7,6},{8,11},{9,8},{10,9... | collective-permute-start | bytes 1572872 | tf_op jit(solution)/shard_map/ppermute | solution.py:34
  140.7 1.8 carry.1
  142.5 10.3 %all-to-all-start.1 = ((bf16[64,16,128]{2,1,0:T(8,128)(2,1)}), bf16[64,16,128]{2,1,0:T(8,128)(2,1)S(1)}, u32[]{:S(2)}, u32[]{:S(2)}) async-start(bf16[64,16,128]{2,1,0:T(8,128)(2,1)} %bitcast.5), calls=%async_computation.1 | async-start | bytes 524288 | tf_op jit(solution)/shard_map/all_to_all | solution.py:512
  152.9 1.2 copy-done.3
  154.1 1.2 copy-done.5
  155.3 1.0 copy-done.11
  156.3 1.0 copy-done.13
  157.4 6.6 %shard_map.221 = (bf16[384,2048]{1,0:T(8,128)(2,1)S(1)}, f32[384,2048]{1,0:T(8,128)S(1)}) custom-call(bf16[7680,128]{1,0:T(8,128)(2,1)S(1)} %bitcast.19, bf16[2048,256]{1,0:T(8,128)(2,1)} %bitcast.9.g0, bf16[2048,256]{1,0:T(8,128)(2,1)S(1)} %bitcast.25, bf16[2048,256]{1,0:T(8,128)(2,1)} %collective-permute-done.4.g1, bf16[2048,256]{1,0:T(8,128)(2,1)S(1)} %copy-done.5, ...), custom_call_target="tpu_custom_call" | custom-call | tf_op jit(solution)/shard_map/pallas_call | solution.py:523
  164.0 2.5 %shard_map.222.hidden_ref = bf16[384,256]{1,0:T(8,128)(2,1)S(1)} custom-call(bf16[384,2048]{1,0:T(8,128)(2,1)S(1)} %get-tuple-element.23.rows_ref, bf16[2048,256]{1,0:T(8,128)(2,1)} %collective-permute-done.12.g, bf16[2048,256]{1,0:T(8,128)(2,1)} %collective-permute-done.13.u), custom_call_target="tpu_custom_call" | custom-call | tf_op jit(solution)/shard_map/pallas_call | solution.py:542
  166.5 4.7 %shard_map.223 = bf16[6144,128]{1,0:T(8,128)(2,1)} custom-call(bf16[384,256]{1,0:T(8,128)(2,1)S(1)} %shard_map.222.hidden_ref, f32[384,2048]{1,0:T(8,128)S(1)} %get-tuple-element.24.sum_ref, bf16[128,2048]{1,0:T(8,128)(2,1)} %collective-permute-done.14.da, bf16[128,2048]{1,0:T(8,128)(2,1)} %collective-permute-done.15.db), custom_call_target="tpu_custom_call" | custom-call | tf_op jit(solution)/shard_map/pallas_call | solution.py:545
  171.3 10.4 %all-to-all-start.2 = ((bf16[64,96,128]{2,1,0:T(8,128)(2,1)}), bf16[64,96,128]{2,1,0:T(8,128)(2,1)S(1)}, u32[]{:S(2)}, u32[]{:S(2)}) async-start(bf16[64,96,128]{2,1,0:T(8,128)(2,1)} %bitcast.14), calls=%async_computation.2 | async-start | bytes 3145728 | tf_op jit(solution)/shard_map/all_to_all | solution.py:551
  181.8 1.0 copy-done.8
  183.4 3.2 %collective-permute-start.18 = (bf16[3072,128]{1,0:T(8,128)(2,1)S(1)}, bf16[3072,128]{1,0:T(8,128)(2,1)S(1)}, u32[]{:S(2)}, u32[]{:S(2)}) collective-permute-start(bf16[3072,128]{1,0:T(8,128)(2,1)S(1)} %shared_pack.1.own), channel_id=1, source_target_pairs={{0,3},{1,0},{2,1},{3,2},{4,7},{5,4},{6,5},{7,6},{8,11},{9,8},{10,9... | collective-permute-start | bytes 2359304 | tf_op jit(solution)/shard_map/ppermute | solution.py:34
  186.6 17.5 %collective-permute-done.17.low = bf16[3072,128]{1,0:T(8,128)(2,1)S(1)} collective-permute-done((bf16[3072,128]{1,0:T(8,128)(2,1)S(1)}, bf16[3072,128]{1,0:T(8,128)(2,1)S(1)}, u32[]{:S(2)}, u32[]{:S(2)}) %collective-permute-start.17) | collective-permute-done | bytes 786464 | tf_op jit(solution)/shard_map/ppermute | solution.py:34
  204.3 2.1 collective-permute-done.16.other_ref
  206.4 17.7 %collective-permute-done.19.far = bf16[3072,128]{1,0:T(8,128)(2,1)S(1)} collective-permute-done((bf16[3072,128]{1,0:T(8,128)(2,1)S(1)}, bf16[3072,128]{1,0:T(8,128)(2,1)S(1)}, u32[]{:S(2)}, u32[]{:S(2)}) %collective-permute-start.19) | collective-permute-done | bytes 786464 | tf_op jit(solution)/shard_map/ppermute | solution.py:34
  224.1 1.0 copy-done.14
  225.1 2.8 %shard_map.224 = (f32[128,2048]{1,0:T(8,128)}, bf16[128,2048]{1,0:T(8,128)(2,1)}) custom-call(bf16[128,2048]{1,0:T(8,128)(2,1)S(1)} %copy-done.14, bf16[128,2048]{1,0:T(8,128)(2,1)S(1)} %collective-permute-done.16.other_ref, bf16[3072,128]{1,0:T(8,128)(2,1)S(1)} %shared_pack.1.own, bf16[3072,128]{1,0:T(8,128)(2,1)S(1)} %collective-permute-done.17.low, ...), custom_call_target="tpu_custom_call" | custom-call | tf_op jit(solution)/shard_map/pallas_call | solution.py:595
  228.3 2.2 copy-done
  230.4 1.9 mixer_out.1
  232.5 1.1 collective-permute-start.2
  233.6 0.9 collective-permute-start.1
  234.5 1.2 convert_add_fusion.shared_ref
  235.7 3.2 %collective-permute-done.3 = bf16[32,2048]{1,0:T(8,128)(2,1)S(1)} collective-permute-done((bf16[32,2048]{1,0:T(8,128)(2,1)S(1)}, bf16[32,2048]{1,0:T(8,128)(2,1)S(1)}, u32[]{:S(2)}, u32[]{:S(2)}) %collective-permute-start.3) | collective-permute-done | bytes 131104 | tf_op jit(solution)/shard_map/ppermute | solution.py:34
  238.8 1.6 collective-permute-done.2
  240.4 2.3 collective-permute-done.1
  242.8 0.7 add_convert_fusion
  243.5 2.5 %shard_map.225 = bf16[128,2048]{1,0:T(8,128)(2,1)} custom-call(bf16[6144,128]{1,0:T(8,128)(2,1)S(1)} %bitcast.20, s32[128,2]{1,0:T(8,128)S(1)} %copy.24.routes_ref, bf16[128,2]{1,0:T(8,128)(2,1)S(1)} %copy.25.scores_ref, f32[128,2048]{1,0:T(8,128)S(1)} %convert_add_fusion.shared_ref), custom_call_target="tpu_custom_call" | custom-call | tf_op jit(solution)/shard_map/pallas_call | solution.py:606
  (64 shorter events, 2.5 us)
Async XLA Ops:
  2.7 5.0 %collective-permute-start = (bf16[3,1280]{1,0:T(4,128)(2,1)S(1)}, bf16[3,1280]{1,0:T(4,128)(2,1)S(1)}, u32[]{:S(2)}, u32[]{:S(2)}) collective-permute-start(bf16[3,1280]{1,0:T(4,128)(2,1)S(1)} %pad_maximum_fusion), channel_id=1, source_target_pairs={{0,4},{4,8},{8,12},{12,16},{16,20},{20,24},{24,28},{28,32},{32,36}... | collective-permute-start | bytes 23048 | tf_op jit(solution)/shard_map/ppermute | solution.py:34
  7.7 0.6 copy-start.20
  14.9 16.4 %copy-start.1 = (bf16[1,256,2048]{2,1,0:T(8,128)(2,1)S(1)}, bf16[1,256,2048]{2,1,0:T(8,128)(2,1)}, u32[]{:S(2)}) copy-start(bf16[1,256,2048]{2,1,0:T(8,128)(2,1)} %param.40) | copy-start | bytes 3145732
  14.9 125.8 %all-to-all-start = ((bf16[64,120,128]{2,1,0:T(8,128)(2,1)}), bf16[64,120,128]{2,1,0:T(8,128)(2,1)S(1)}, u32[]{:S(2)}, u32[]{:S(2)}) async-start(bf16[64,120,128]{2,1,0:T(8,128)(2,1)} %bitcast.27), calls=%async_computation | async-start | bytes 3932160 | tf_op jit(solution)/shard_map/all_to_all | solution.py:483
  28.0 38.9 %copy-start.2 = (bf16[1,2048,256]{2,1,0:T(8,128)(2,1)S(1)}, bf16[1,2048,256]{2,1,0:T(8,128)(2,1)}, u32[]{:S(2)}) copy-start(bf16[1,2048,256]{2,1,0:T(8,128)(2,1)} %param.39) | copy-start | bytes 3145732
  28.0 52.6 %collective-permute-start.4 = (bf16[2048,256]{1,0:T(8,128)(2,1)}, bf16[2048,256]{1,0:T(8,128)(2,1)}, u32[]{:S(2)}, u32[]{:S(2)}) collective-permute-start(bf16[2048,256]{1,0:T(8,128)(2,1)} %bitcast.9.g0), channel_id=1, source_target_pairs={{0,1},{1,2},{2,3},{3,0},{4,5},{5,6},{6,7},{7,4},{8,9},{9,10},{10,1... | collective-permute-start | bytes 3145736 | tf_op jit(solution)/shard_map/ppermute | solution.py:34
  29.6 51.2 %collective-permute-start.7 = (bf16[2048,256]{1,0:T(8,128)(2,1)}, bf16[2048,256]{1,0:T(8,128)(2,1)}, u32[]{:S(2)}, u32[]{:S(2)}) collective-permute-start(bf16[2048,256]{1,0:T(8,128)(2,1)} %bitcast.23), channel_id=1, source_target_pairs={{0,3},{1,0},{2,1},{3,2},{4,7},{5,4},{6,5},{7,6},{8,11},{9,8},{10,9... | collective-permute-start | bytes 3145736 | tf_op jit(solution)/shard_map/ppermute | solution.py:34
  31.4 35.4 %collective-permute-start.8 = (bf16[128,2048]{1,0:T(8,128)(2,1)S(1)}, bf16[128,2048]{1,0:T(8,128)(2,1)}, u32[]{:S(2)}, u32[]{:S(2)}) collective-permute-start(bf16[128,2048]{1,0:T(8,128)(2,1)S(1)} %get-tuple-element.29), channel_id=1, source_target_pairs={{0,1},{1,2},{2,3},{3,0},{4,5},{5,6},{6,7},{7,4},{8,9},{9,10},{10,1... | collective-permute-start | bytes 1572872 | tf_op jit(solution)/shard_map/ppermute | solution.py:34
  31.9 46.1 %collective-permute-start.9 = (bf16[128,2048]{1,0:T(8,128)(2,1)S(1)}, bf16[128,2048]{1,0:T(8,128)(2,1)S(1)}, u32[]{:S(2)}, u32[]{:S(2)}) collective-permute-start(bf16[128,2048]{1,0:T(8,128)(2,1)S(1)} %get-tuple-element.28), channel_id=1, source_target_pairs={{0,1},{1,2},{2,3},{3,0},{4,5},{5,6},{6,7},{7,4},{8,9},{9,10},{10,1... | collective-permute-start | bytes 1572872 | tf_op jit(solution)/shard_map/ppermute | solution.py:34
  33.4 50.4 %collective-permute-start.10 = (bf16[128,2048]{1,0:T(8,128)(2,1)S(1)}, bf16[128,2048]{1,0:T(8,128)(2,1)S(1)}, u32[]{:S(2)}, u32[]{:S(2)}) collective-permute-start(bf16[128,2048]{1,0:T(8,128)(2,1)S(1)} %get-tuple-element.29), channel_id=1, source_target_pairs={{0,3},{1,0},{2,1},{3,2},{4,7},{5,4},{6,5},{7,6},{8,11},{9,8},{10,9... | collective-permute-start | bytes 1572872 | tf_op jit(solution)/shard_map/ppermute | solution.py:34
  66.9 69.8 %collective-permute-start.5 = (bf16[2048,256]{1,0:T(8,128)(2,1)S(1)}, bf16[2048,256]{1,0:T(8,128)(2,1)S(1)}, u32[]{:S(2)}, u32[]{:S(2)}) collective-permute-start(bf16[2048,256]{1,0:T(8,128)(2,1)S(1)} %bitcast.24), channel_id=1, source_target_pairs={{0,1},{1,2},{2,3},{3,0},{4,5},{5,6},{6,7},{7,4},{8,9},{9,10},{10,1... | collective-permute-start | bytes 3145736 | tf_op jit(solution)/shard_map/ppermute | solution.py:34
  78.0 0.8 copy-start.10
  78.8 74.0 %collective-permute-start.6 = (bf16[2048,256]{1,0:T(8,128)(2,1)}, bf16[2048,256]{1,0:T(8,128)(2,1)}, u32[]{:S(2)}, u32[]{:S(2)}) collective-permute-start(bf16[2048,256]{1,0:T(8,128)(2,1)} %bitcast.9.g0), channel_id=1, source_target_pairs={{0,3},{1,0},{2,1},{3,2},{4,7},{5,4},{6,5},{7,6},{8,11},{9,8},{10,9... | collective-permute-start | bytes 3145736 | tf_op jit(solution)/shard_map/ppermute | solution.py:34
  80.6 83.4 %collective-permute-start.12 = (bf16[2048,256]{1,0:T(8,128)(2,1)}, bf16[2048,256]{1,0:T(8,128)(2,1)}, u32[]{:S(2)}, u32[]{:S(2)}) collective-permute-start(bf16[2048,256]{1,0:T(8,128)(2,1)} %collective-permute-done.4.g1), channel_id=1, source_target_pairs={{0,1},{1,2},{2,3},{3,0},{4,5},{5,6},{6,7},{7,4},{8,9},{9,10},{10,1... | collective-permute-start | bytes 3145736 | tf_op jit(solution)/shard_map/ppermute | solution.py:34
  80.8 83.1 %collective-permute-start.13 = (bf16[2048,256]{1,0:T(8,128)(2,1)}, bf16[2048,256]{1,0:T(8,128)(2,1)}, u32[]{:S(2)}, u32[]{:S(2)}) collective-permute-start(bf16[2048,256]{1,0:T(8,128)(2,1)} %collective-permute-done.7.u2), channel_id=1, source_target_pairs={{0,3},{1,0},{2,1},{3,2},{4,7},{5,4},{6,5},{7,6},{8,11},{9,8},{10,9... | collective-permute-start | bytes 3145736 | tf_op jit(solution)/shard_map/ppermute | solution.py:34
  83.8 0.8 copy-start.12
  84.6 51.8 %collective-permute-start.11 = (bf16[128,2048]{1,0:T(8,128)(2,1)S(1)}, bf16[128,2048]{1,0:T(8,128)(2,1)}, u32[]{:S(2)}, u32[]{:S(2)}) collective-permute-start(bf16[128,2048]{1,0:T(8,128)(2,1)S(1)} %get-tuple-element.28), channel_id=1, source_target_pairs={{0,3},{1,0},{2,1},{3,2},{4,7},{5,4},{6,5},{7,6},{8,11},{9,8},{10,9... | collective-permute-start | bytes 1572872 | tf_op jit(solution)/shard_map/ppermute | solution.py:34
  136.4 30.1 %collective-permute-start.14 = (bf16[128,2048]{1,0:T(8,128)(2,1)}, bf16[128,2048]{1,0:T(8,128)(2,1)}, u32[]{:S(2)}, u32[]{:S(2)}) collective-permute-start(bf16[128,2048]{1,0:T(8,128)(2,1)} %collective-permute-done.8.d1a), channel_id=1, source_target_pairs={{0,1},{1,2},{2,3},{3,0},{4,5},{5,6},{6,7},{7,4},{8,9},{9,10},{10,1... | collective-permute-start | bytes 1572872 | tf_op jit(solution)/shard_map/ppermute | solution.py:34
  136.7 1.0 copy-start.4
  137.7 28.8 %collective-permute-start.15 = (bf16[128,2048]{1,0:T(8,128)(2,1)}, bf16[128,2048]{1,0:T(8,128)(2,1)}, u32[]{:S(2)}, u32[]{:S(2)}) collective-permute-start(bf16[128,2048]{1,0:T(8,128)(2,1)} %collective-permute-done.11.d2b), channel_id=1, source_target_pairs={{0,3},{1,0},{2,1},{3,2},{4,7},{5,4},{6,5},{7,6},{8,11},{9,8},{10,9... | collective-permute-start | bytes 1572872 | tf_op jit(solution)/shard_map/ppermute | solution.py:34
  142.5 28.8 %all-to-all-start.1 = ((bf16[64,16,128]{2,1,0:T(8,128)(2,1)}), bf16[64,16,128]{2,1,0:T(8,128)(2,1)S(1)}, u32[]{:S(2)}, u32[]{:S(2)}) async-start(bf16[64,16,128]{2,1,0:T(8,128)(2,1)} %bitcast.5), calls=%async_computation.1 | async-start | bytes 524288 | tf_op jit(solution)/shard_map/all_to_all | solution.py:512
  152.8 1.2 copy-start.3
  154.1 1.2 copy-start.5
  155.3 1.0 copy-start.11
  156.3 1.0 copy-start.13
  171.3 10.5 %copy-start.6 = (bf16[2048,128]{1,0:T(8,128)(2,1)S(1)}, bf16[2048,128]{1,0:T(8,128)(2,1)}, u32[]{:S(2)}) copy-start(bf16[2048,128]{1,0:T(8,128)(2,1)} %gate_ref.3) | copy-start | bytes 1572868
  171.3 10.5 %copy-start.7 = (bf16[2048,128]{1,0:T(8,128)(2,1)S(1)}, bf16[2048,128]{1,0:T(8,128)(2,1)}, u32[]{:S(2)}) copy-start(bf16[2048,128]{1,0:T(8,128)(2,1)} %up_ref.1) | copy-start | bytes 1572868
  171.3 72.2 %all-to-all-start.2 = ((bf16[64,96,128]{2,1,0:T(8,128)(2,1)}), bf16[64,96,128]{2,1,0:T(8,128)(2,1)S(1)}, u32[]{:S(2)}, u32[]{:S(2)}) async-start(bf16[64,96,128]{2,1,0:T(8,128)(2,1)} %bitcast.14), calls=%async_computation.2 | async-start | bytes 3145728 | tf_op jit(solution)/shard_map/all_to_all | solution.py:551
  181.8 1.0 copy-start.8
  183.3 20.9 %collective-permute-start.17 = (bf16[3072,128]{1,0:T(8,128)(2,1)S(1)}, bf16[3072,128]{1,0:T(8,128)(2,1)S(1)}, u32[]{:S(2)}, u32[]{:S(2)}) collective-permute-start(bf16[3072,128]{1,0:T(8,128)(2,1)S(1)} %shared_pack.1.own), channel_id=1, source_target_pairs={{0,1},{1,2},{2,3},{3,0},{4,5},{5,6},{6,7},{7,4},{8,9},{9,10},{10,1... | collective-permute-start | bytes 2359304 | tf_op jit(solution)/shard_map/ppermute | solution.py:34
  183.4 23.0 %collective-permute-start.18 = (bf16[3072,128]{1,0:T(8,128)(2,1)S(1)}, bf16[3072,128]{1,0:T(8,128)(2,1)S(1)}, u32[]{:S(2)}, u32[]{:S(2)}) collective-permute-start(bf16[3072,128]{1,0:T(8,128)(2,1)S(1)} %shared_pack.1.own), channel_id=1, source_target_pairs={{0,3},{1,0},{2,1},{3,2},{4,7},{5,4},{6,5},{7,6},{8,11},{9,8},{10,9... | collective-permute-start | bytes 2359304 | tf_op jit(solution)/shard_map/ppermute | solution.py:34
  204.1 19.9 %collective-permute-start.19 = (bf16[3072,128]{1,0:T(8,128)(2,1)S(1)}, bf16[3072,128]{1,0:T(8,128)(2,1)S(1)}, u32[]{:S(2)}, u32[]{:S(2)}) collective-permute-start(bf16[3072,128]{1,0:T(8,128)(2,1)S(1)} %collective-permute-done.17.low), channel_id=1, source_target_pairs={{0,1},{1,2},{2,3},{3,0},{4,5},{5,6},{6,7},{7,4},{8,9},{9,10},{10,1... | collective-permute-start | bytes 2359304 | tf_op jit(solution)/shard_map/ppermute | solution.py:34
  204.1 23.8 %copy-start.21 = (s32[128,2]{0,1:T(2,128)S(1)}, s32[128,2]{0,1:T(2,128)}, u32[]{:S(2)}) copy-start(s32[128,2]{0,1:T(2,128)} %param.36) | copy-start | bytes 3076
  204.1 23.9 %copy-start.22 = (bf16[128,2]{0,1:T(2,128)(2,1)S(1)}, bf16[128,2]{0,1:T(2,128)(2,1)}, u32[]{:S(2)}) copy-start(bf16[128,2]{0,1:T(2,128)(2,1)} %param.37) | copy-start | bytes 1540
  204.1 24.1 %copy-start.9 = (f32[128,1024]{1,0:T(8,128)S(1)}, f32[128,1024]{1,0:T(8,128)}, u32[]{:S(2)}) copy-start(f32[128,1024]{1,0:T(8,128)} %get-tuple-element.18.local_ref) | copy-start | bytes 1572868
  204.2 2.2 collective-permute-start.16
  224.1 1.0 copy-start.14
  225.1 3.1 %copy-start.15 = (bf16[128,1024]{1,0:T(8,128)(2,1)S(1)}, bf16[128,1024]{1,0:T(8,128)(2,1)}, u32[]{:S(2)}) copy-start(bf16[128,1024]{1,0:T(8,128)(2,1)} %gate_ref.2) | copy-start | bytes 786436
  225.1 3.1 %copy-start.16 = (f32[128,128]{1,0:T(8,128)S(1)}, f32[128,128]{1,0:T(8,128)}, u32[]{:S(2)}) copy-start(f32[128,128]{1,0:T(8,128)} %get-tuple-element.16.read_ref) | copy-start | bytes 196612
  225.1 3.1 %copy-start.17 = (f32[128,16]{1,0:T(8,128)S(1)}, f32[128,16]{1,0:T(8,128)}, u32[]{:S(2)}) copy-start(f32[128,16]{1,0:T(8,128)} %get-tuple-element.17.grow_ref) | copy-start | bytes 24580
  225.1 3.1 %copy-start.18 = (f32[1024]{0:T(1024)S(1)}, f32[1024]{0:T(1024)}, u32[]{:S(2)}) copy-start(f32[1024]{0:T(1024)} %param.32) | copy-start | bytes 12292
  228.0 6.5 %collective-permute-start.20 = (bf16[128,2048]{1,0:T(8,128)(2,1)}, bf16[128,2048]{1,0:T(8,128)(2,1)}, u32[]{:S(2)}, u32[]{:S(2)}) collective-permute-start(bf16[128,2048]{1,0:T(8,128)(2,1)} %get-tuple-element.27), channel_id=1, source_target_pairs={{0,4},{4,0},{1,5},{5,1},{2,6},{6,2},{3,7},{7,3},{8,12},{12,8},{9,1... | collective-permute-start | bytes 1572872 | tf_op jit(solution)/shard_map/ppermute | solution.py:34
  228.3 2.2 copy-start
  230.4 4.0 %copy-start.19 = (f32[128,2048]{1,0:T(8,128)S(1)}, f32[128,2048]{1,0:T(8,128)}, u32[]{:S(2)}) copy-start(f32[128,2048]{1,0:T(8,128)} %get-tuple-element.26) | copy-start | bytes 3145732
  232.4 6.4 %collective-permute-start.3 = (bf16[32,2048]{1,0:T(8,128)(2,1)S(1)}, bf16[32,2048]{1,0:T(8,128)(2,1)S(1)}, u32[]{:S(2)}, u32[]{:S(2)}) collective-permute-start(bf16[32,2048]{1,0:T(8,128)(2,1)S(1)} %get-tuple-element.22), channel_id=1, source_target_pairs={{0,3},{1,0},{2,1},{3,2},{4,7},{5,4},{6,5},{7,6},{8,11},{9,8},{10,9... | collective-permute-start | bytes 393224 | tf_op jit(solution)/shard_map/ppermute | solution.py:34
  232.5 8.0 %collective-permute-start.2 = (bf16[32,2048]{1,0:T(8,128)(2,1)S(1)}, bf16[32,2048]{1,0:T(8,128)(2,1)S(1)}, u32[]{:S(2)}, u32[]{:S(2)}) collective-permute-start(bf16[32,2048]{1,0:T(8,128)(2,1)S(1)} %get-tuple-element.21), channel_id=1, source_target_pairs={{0,2},{1,3},{2,0},{3,1},{4,6},{5,7},{6,4},{7,5},{8,10},{9,11},{10,... | collective-permute-start | bytes 393224 | tf_op jit(solution)/shard_map/ppermute | solution.py:34
  233.6 9.2 %collective-permute-start.1 = (bf16[32,2048]{1,0:T(8,128)(2,1)S(1)}, bf16[32,2048]{1,0:T(8,128)(2,1)S(1)}, u32[]{:S(2)}, u32[]{:S(2)}) collective-permute-start(bf16[32,2048]{1,0:T(8,128)(2,1)S(1)} %get-tuple-element.20), channel_id=1, source_target_pairs={{0,1},{1,2},{2,3},{3,0},{4,5},{5,6},{6,7},{7,4},{8,9},{9,10},{10,1... | collective-permute-start | bytes 393224 | tf_op jit(solution)/shard_map/ppermute | solution.py:34

commit v3 on v2

--- a/solution.py
+++ b/solution.py
@@ -109,27 +109,52 @@
     hidden_ref[...] = expert_hidden(rows_ref[...], g[...], u[...])
 
 
-def expert_last_body(capacity, hidden_ref, sum_ref, da, db, out_ref, scr):
+def expert_last_body(
+    capacity, hidden_ref, sum_ref, da, db, out_ref, held_a, held_b, packed, scr, in_sems, out_sems
+):
     slots, width = sum_ref.shape
     pieces = width // LANE
+    parts = in_sems.shape[0] // 2
+    span = width // parts
+    arriving = []
+    for i in range(parts):
+        for j, (source, target) in enumerate(((da, held_a), (db, held_b))):
+            cols = pl.ds(i * span, span)
+            arriving.append(
+                pltpu.make_async_copy(source.at[:, cols], target.at[:, cols], in_sems.at[2 * i + j])
+            )
+    for copy in arriving:
+        copy.start()
     hidden = hidden_ref[...]
+    sources = slots // capacity
     for k in range(0, pieces, 2):
+        if k * LANE % span == 0:
+            first = 2 * (k * LANE // span)
+            arriving[first].wait()
+            arriving[first + 1].wait()
         cols = slice(k * LANE, (k + 2) * LANE)
-        part = (
-            sum_ref[:, cols]
-            + jnp.dot(
-                hidden,
-                jnp.concatenate([da[:, cols], db[:, cols]], axis=0),
-                preferred_element_type=f32,
-            )
+        part = sum_ref[:, cols] + jnp.dot(
+            hidden,
+            jnp.concatenate([held_a[:, cols], held_b[:, cols]], axis=0),
+            preferred_element_type=f32,
         )
-        sources = slots // capacity
         for r in range(capacity):
             own = part[r * sources : (r + 1) * sources, :]
             row = r * pieces + k
             scr[pl.ds(row, sources, stride=capacity * pieces), :] = own[:, :LANE]
             scr[pl.ds(row + 1, sources, stride=capacity * pieces), :] = own[:, LANE:]
-    out_ref[...] = scr[...].astype(bf16)
+    count = out_sems.shape[0]
+    chunk = packed.shape[0] // count
+    leaving = []
+    for i in range(count):
+        packed[i * chunk : (i + 1) * chunk, :] = scr[i * chunk : (i + 1) * chunk, :].astype(bf16)
+        rows = pl.ds(i * chunk, chunk)
+        leaving.append(
+            pltpu.make_async_copy(packed.at[rows, :], out_ref.at[rows, :], out_sems.at[i])
+        )
+        leaving[-1].start()
+    for copy in leaving:
+        copy.wait()
 
 
 def shared_pack_body(core_ref, gate_ref, up_ref, down_ref, out_ref):
@@ -517,9 +542,7 @@
     high_gate, high_up, high_down_a, high_down_b = map(
         keep_near, (high_gate, high_up, high_down_a, high_down_b)
     )
-    far_gate, far_up, far_down_a, far_down_b = map(
-        keep_near, (far_gate, far_up, far_down_a, far_down_b)
-    )
+    far_gate, far_up = map(keep_near, (far_gate, far_up))
     expert_rows, expert_sum = call(
         functools.partial(expert_first_body, capacity, chunk_rows),
         (pltpu.VMEM((slots, width), bf16), pltpu.VMEM((slots, width), f32)),
@@ -542,11 +565,22 @@
     far_hidden = call(
         expert_hidden_body, jax.ShapeDtypeStruct((slots, down.shape[0]), bf16), (), 10
     )(expert_rows, far_gate, far_up)
-    sent_back = call(
+    in_vmem = pl.BlockSpec(memory_space=pltpu.VMEM)
+    sent_back = pl.pallas_call(
         functools.partial(expert_last_body, capacity),
-        jax.ShapeDtypeStruct((slots * pieces, LANE), bf16),
-        [pltpu.VMEM((slots * pieces, LANE), f32)],
-        14,
+        out_shape=pltpu.HBM((slots * pieces, LANE), bf16),
+        in_specs=[in_vmem, in_vmem, in_hbm, in_hbm],
+        out_specs=in_hbm,
+        scratch_shapes=[
+            pltpu.VMEM((half, width), bf16),
+            pltpu.VMEM((half, width), bf16),
+            pltpu.VMEM((slots * pieces, LANE), bf16),
+            pltpu.VMEM((slots * pieces, LANE), f32),
+            pltpu.SemaphoreType.DMA((8,)),
+            pltpu.SemaphoreType.DMA((4,)),
+        ],
+        compiler_params=pltpu.CompilerParams(vmem_limit_bytes=16 * MIB),
+        name="experts_last",
     )(far_hidden, expert_sum, far_down_a, far_down_b)
     returned = lax.all_to_all(sent_back.reshape(exchanged), EP, 0, 0, tiled=True)
 

time: 248 us -> 248 us (level)
  transfers between devices with their start and end apart: 24 -> 24, of which waited for: 10 -> 10; matrix products, arithmetic and copies ran while one was open for 1% -> 1% of each run, Pallas kernels for 8% -> 9%
where the time goes in v3:
time: 248 us; the launch traced here: 247 us
  waiting for transfers between devices  142 us (57%)
  starting transfers between devices  57.1 us (23%)
  Pallas kernels  30.2 us (12%)
  local copies, waits for them, and re-layouts  14.5 us (6%)
    ppermute x21, waiting for transfers between devices, shift(): return lax.ppermute(value, axis, pairs)  142 us
    ppermute x21, starting transfers between devices, shift(): return lax.ppermute(value, axis, pairs)  23.3 us
    all_to_all x1, starting transfers between devices, layer(): lax.all_to_all(sent.reshape(experts, chunk_rows, LANE), EP, 0, 0, tiled=T...  13 us
    unnamed x48, local copies, waits for them, and re-layouts  12.3 us
    all_to_all x1, starting transfers between devices, layer(): lax.all_to_all(sent_back.reshape(exchanged), EP, 0, 0, tiled=True)  10.4 us
    all_to_all x1, starting transfers between devices, layer(): lax.all_to_all(entering.reshape(ep_count, 16, STATE), EP, 0, 0, tiled=True)  10.3 us
    pallas_call x1, Pallas kernels, layer(): pl.pallas_call(functools.partial(front_body, capacity, experts, chunk_row...  6.59 us
    pallas_call x1, Pallas kernels, layer(): call(functools.partial(expert_first_body, capacity, chunk_rows), (pltpu.V...  6.56 us
  transfers between devices with their start and end apart: 24, of which 10 were waited for; matrix products, arithmetic and copies ran while one was open for 1% of the time, Pallas kernels for 9%

profile of v3, /device:TPU:2, one launch (start us, length us, event | category | flops | bytes accessed | tf_op | source)
XLA Modules:
  0.0 246.5 jit_solution(14399444099274916018)
XLA Ops:
  0.6 0.7 slice.23
  1.3 0.7 slice.22
  2.0 0.7 slice.21
  2.7 1.9 collective-permute-start
  4.7 3.1 %collective-permute-done.refs_6_ = bf16[3,1280]{1,0:T(4,128)(2,1)S(1)} collective-permute-done((bf16[3,1280]{1,0:T(4,128)(2,1)S(1)}, bf16[3,1280]{1,0:T(4,128)(2,1)S(1)}, u32[]{:S(2)}, u32[]{:S(2)}) %collective-permute-start) | collective-permute-done | bytes 7712 | tf_op jit(solution)/shard_map/ppermute | solution.py:34
  7.7 0.6 copy-done.20
  8.3 6.6 %front.1 = (bf16[128,2048]{1,0:T(8,128)(2,1)}, bf16[7680,128]{1,0:T(8,128)(2,1)}, f32[128,1024]{1,0:T(8,128)}, f32[128,128]{1,0:T(8,128)}, f32[128,16]{1,0:T(8,128)}) custom-call(bf16[128,2048]{1,0:T(8,128)(2,1)} %refs_0_.1, f32[1,2048]{1,0:T(1,128)} %bitcast.29, s32[2,128]{1,0:T(2,128)} %bitcast.30, bf16[128,1024]{1,0:T(8,128)(2,1)} %refs_3_.1, ...), custom_call_target="tpu_custom_call" | custom-call | tf_op jit(solution)/shard_map/front/pallas_call | solution.py:492
  14.9 13.0 %all-to-all-start = ((bf16[64,120,128]{2,1,0:T(8,128)(2,1)}), bf16[64,120,128]{2,1,0:T(8,128)(2,1)S(1)}, u32[]{:S(2)}, u32[]{:S(2)}) async-start(bf16[64,120,128]{2,1,0:T(8,128)(2,1)} %bitcast.28), calls=%async_computation | async-start | bytes 3932160 | tf_op jit(solution)/shard_map/all_to_all | solution.py:508
  28.0 1.7 collective-permute-start.4
  29.6 1.7 collective-permute-start.7
  31.9 1.6 collective-permute-start.9
  33.4 1.7 collective-permute-start.10
  35.1 31.8 %collective-permute-done.8.d1a = bf16[128,2048]{1,0:T(8,128)(2,1)} collective-permute-done((bf16[128,2048]{1,0:T(8,128)(2,1)S(1)}, bf16[128,2048]{1,0:T(8,128)(2,1)}, u32[]{:S(2)}, u32[]{:S(2)}) %collective-permute-start.8) | collective-permute-done | bytes 524320 | tf_op jit(solution)/shard_map/ppermute | solution.py:34
  67.2 10.8 %collective-permute-done.9.d1b = bf16[128,2048]{1,0:T(8,128)(2,1)S(1)} collective-permute-done((bf16[128,2048]{1,0:T(8,128)(2,1)S(1)}, bf16[128,2048]{1,0:T(8,128)(2,1)S(1)}, u32[]{:S(2)}, u32[]{:S(2)}) %collective-permute-start.9) | collective-permute-done | bytes 524320 | tf_op jit(solution)/shard_map/ppermute | solution.py:34
  78.0 0.8 copy-done.10
  78.8 1.8 collective-permute-start.6
  80.8 3.0 %collective-permute-start.13 = (bf16[2048,256]{1,0:T(8,128)(2,1)}, bf16[2048,256]{1,0:T(8,128)(2,1)}, u32[]{:S(2)}, u32[]{:S(2)}) collective-permute-start(bf16[2048,256]{1,0:T(8,128)(2,1)} %collective-permute-done.7.u2), channel_id=1, source_target_pairs={{0,3},{1,0},{2,1},{3,2},{4,7},{5,4},{6,5},{7,6},{8,11},{9,8},{10,9... | collective-permute-start | bytes 3145736 | tf_op jit(solution)/shard_map/ppermute | solution.py:34
  83.8 0.8 copy-done.12
  84.6 51.8 %collective-permute-done.11.d2b = bf16[128,2048]{1,0:T(8,128)(2,1)} collective-permute-done((bf16[128,2048]{1,0:T(8,128)(2,1)S(1)}, bf16[128,2048]{1,0:T(8,128)(2,1)}, u32[]{:S(2)}, u32[]{:S(2)}) %collective-permute-start.11) | collective-permute-done | bytes 524320 | tf_op jit(solution)/shard_map/ppermute | solution.py:34
  136.7 1.0 copy-done.4
  137.7 3.0 %collective-permute-start.15 = (bf16[128,2048]{1,0:T(8,128)(2,1)}, bf16[128,2048]{1,0:T(8,128)(2,1)}, u32[]{:S(2)}, u32[]{:S(2)}) collective-permute-start(bf16[128,2048]{1,0:T(8,128)(2,1)} %collective-permute-done.11.d2b), channel_id=1, source_target_pairs={{0,3},{1,0},{2,1},{3,2},{4,7},{5,4},{6,5},{7,6},{8,11},{9,8},{10,9... | collective-permute-start | bytes 1572872 | tf_op jit(solution)/shard_map/ppermute | solution.py:34
  140.7 1.8 carry.1
  142.5 10.3 %all-to-all-start.1 = ((bf16[64,16,128]{2,1,0:T(8,128)(2,1)}), bf16[64,16,128]{2,1,0:T(8,128)(2,1)S(1)}, u32[]{:S(2)}, u32[]{:S(2)}) async-start(bf16[64,16,128]{2,1,0:T(8,128)(2,1)} %bitcast.5), calls=%async_computation.1 | async-start | bytes 524288 | tf_op jit(solution)/shard_map/all_to_all | solution.py:537
  152.9 1.2 copy-done.3
  154.1 1.2 copy-done.5
  155.3 1.0 copy-done.11
  156.3 1.0 copy-done.13
  157.4 6.6 %shard_map.221 = (bf16[384,2048]{1,0:T(8,128)(2,1)S(1)}, f32[384,2048]{1,0:T(8,128)S(1)}) custom-call(bf16[7680,128]{1,0:T(8,128)(2,1)S(1)} %bitcast.19, bf16[2048,256]{1,0:T(8,128)(2,1)} %bitcast.9.g0, bf16[2048,256]{1,0:T(8,128)(2,1)S(1)} %bitcast.25, bf16[2048,256]{1,0:T(8,128)(2,1)} %collective-permute-done.4.g1, bf16[2048,256]{1,0:T(8,128)(2,1)S(1)} %copy-done.5, ...), custom_call_target="tpu_custom_call" | custom-call | tf_op jit(solution)/shard_map/pallas_call | solution.py:546
  164.0 2.5 %shard_map.222.hidden_ref = bf16[384,256]{1,0:T(8,128)(2,1)S(1)} custom-call(bf16[384,2048]{1,0:T(8,128)(2,1)S(1)} %get-tuple-element.23.rows_ref, bf16[2048,256]{1,0:T(8,128)(2,1)} %collective-permute-done.12.g, bf16[2048,256]{1,0:T(8,128)(2,1)} %collective-permute-done.13.u), custom_call_target="tpu_custom_call" | custom-call | tf_op jit(solution)/shard_map/pallas_call | solution.py:565
  166.5 5.0 %experts_last.1 = bf16[6144,128]{1,0:T(8,128)(2,1)} custom-call(bf16[384,256]{1,0:T(8,128)(2,1)S(1)} %shard_map.222.hidden_ref, f32[384,2048]{1,0:T(8,128)S(1)} %get-tuple-element.24.sum_ref, bf16[128,2048]{1,0:T(8,128)(2,1)} %collective-permute-done.14.da, bf16[128,2048]{1,0:T(8,128)(2,1)} %collective-permute-done.15.db), custom_call_target="tpu_custom_call" | custom-call | tf_op jit(solution)/shard_map/experts_last/pallas_call | solution.py:569
  171.6 10.4 %all-to-all-start.2 = ((bf16[64,96,128]{2,1,0:T(8,128)(2,1)}), bf16[64,96,128]{2,1,0:T(8,128)(2,1)S(1)}, u32[]{:S(2)}, u32[]{:S(2)}) async-start(bf16[64,96,128]{2,1,0:T(8,128)(2,1)} %bitcast.27), calls=%async_computation.2 | async-start | bytes 3145728 | tf_op jit(solution)/shard_map/all_to_all | solution.py:585
  182.0 1.0 copy-done.8
  183.9 3.2 %collective-permute-start.18 = (bf16[3072,128]{1,0:T(8,128)(2,1)S(1)}, bf16[3072,128]{1,0:T(8,128)(2,1)S(1)}, u32[]{:S(2)}, u32[]{:S(2)}) collective-permute-start(bf16[3072,128]{1,0:T(8,128)(2,1)S(1)} %shared_pack.1.own), channel_id=1, source_target_pairs={{0,3},{1,0},{2,1},{3,2},{4,7},{5,4},{6,5},{7,6},{8,11},{9,8},{10,9... | collective-permute-start | bytes 2359304 | tf_op jit(solution)/shard_map/ppermute | solution.py:34
  187.1 17.5 %collective-permute-done.17.low = bf16[3072,128]{1,0:T(8,128)(2,1)S(1)} collective-permute-done((bf16[3072,128]{1,0:T(8,128)(2,1)S(1)}, bf16[3072,128]{1,0:T(8,128)(2,1)S(1)}, u32[]{:S(2)}, u32[]{:S(2)}) %collective-permute-start.17) | collective-permute-done | bytes 786464 | tf_op jit(solution)/shard_map/ppermute | solution.py:34
  204.7 2.1 collective-permute-done.16.other_ref
  206.8 17.7 %collective-permute-done.19.far = bf16[3072,128]{1,0:T(8,128)(2,1)S(1)} collective-permute-done((bf16[3072,128]{1,0:T(8,128)(2,1)S(1)}, bf16[3072,128]{1,0:T(8,128)(2,1)S(1)}, u32[]{:S(2)}, u32[]{:S(2)}) %collective-permute-start.19) | collective-permute-done | bytes 786464 | tf_op jit(solution)/shard_map/ppermute | solution.py:34
  224.5 1.0 copy-done.14
  225.6 2.8 %shard_map.223 = (f32[128,2048]{1,0:T(8,128)}, bf16[128,2048]{1,0:T(8,128)(2,1)}) custom-call(bf16[128,2048]{1,0:T(8,128)(2,1)S(1)} %copy-done.14, bf16[128,2048]{1,0:T(8,128)(2,1)S(1)} %collective-permute-done.16.other_ref, bf16[3072,128]{1,0:T(8,128)(2,1)S(1)} %shared_pack.1.own, bf16[3072,128]{1,0:T(8,128)(2,1)S(1)} %collective-permute-done.17.low, ...), custom_call_target="tpu_custom_call" | custom-call | tf_op jit(solution)/shard_map/pallas_call | solution.py:629
  228.7 2.2 copy-done
  230.9 1.9 mixer_out.1
  232.9 1.1 collective-permute-start.2
  234.1 0.9 collective-permute-start.1
  235.0 1.2 convert_add_fusion.shared_ref
  236.1 3.1 %collective-permute-done.3 = bf16[32,2048]{1,0:T(8,128)(2,1)S(1)} collective-permute-done((bf16[32,2048]{1,0:T(8,128)(2,1)S(1)}, bf16[32,2048]{1,0:T(8,128)(2,1)S(1)}, u32[]{:S(2)}, u32[]{:S(2)}) %collective-permute-start.3) | collective-permute-done | bytes 131104 | tf_op jit(solution)/shard_map/ppermute | solution.py:34
  239.3 1.6 collective-permute-done.2
  240.9 2.3 collective-permute-done.1
  243.3 0.7 add_convert_fusion
  244.0 2.5 %shard_map.224 = bf16[128,2048]{1,0:T(8,128)(2,1)} custom-call(bf16[6144,128]{1,0:T(8,128)(2,1)S(1)} %bitcast.20, s32[128,2]{1,0:T(8,128)S(1)} %copy.24.routes_ref, bf16[128,2]{1,0:T(8,128)(2,1)S(1)} %copy.25.scores_ref, f32[128,2048]{1,0:T(8,128)S(1)} %convert_add_fusion.shared_ref), custom_call_target="tpu_custom_call" | custom-call | tf_op jit(solution)/shard_map/pallas_call | solution.py:640
  (64 shorter events, 2.7 us)
Async XLA Ops:
  2.7 5.0 %collective-permute-start = (bf16[3,1280]{1,0:T(4,128)(2,1)S(1)}, bf16[3,1280]{1,0:T(4,128)(2,1)S(1)}, u32[]{:S(2)}, u32[]{:S(2)}) collective-permute-start(bf16[3,1280]{1,0:T(4,128)(2,1)S(1)} %pad_maximum_fusion), channel_id=1, source_target_pairs={{0,4},{4,8},{8,12},{12,16},{16,20},{20,24},{24,28},{28,32},{32,36}... | collective-permute-start | bytes 23048 | tf_op jit(solution)/shard_map/ppermute | solution.py:34
  7.7 0.6 copy-start.20
  14.9 16.4 %copy-start.1 = (bf16[1,256,2048]{2,1,0:T(8,128)(2,1)S(1)}, bf16[1,256,2048]{2,1,0:T(8,128)(2,1)}, u32[]{:S(2)}) copy-start(bf16[1,256,2048]{2,1,0:T(8,128)(2,1)} %param.40) | copy-start | bytes 3145732
  14.9 125.8 %all-to-all-start = ((bf16[64,120,128]{2,1,0:T(8,128)(2,1)}), bf16[64,120,128]{2,1,0:T(8,128)(2,1)S(1)}, u32[]{:S(2)}, u32[]{:S(2)}) async-start(bf16[64,120,128]{2,1,0:T(8,128)(2,1)} %bitcast.28), calls=%async_computation | async-start | bytes 3932160 | tf_op jit(solution)/shard_map/all_to_all | solution.py:508
  28.0 38.9 %copy-start.2 = (bf16[1,2048,256]{2,1,0:T(8,128)(2,1)S(1)}, bf16[1,2048,256]{2,1,0:T(8,128)(2,1)}, u32[]{:S(2)}) copy-start(bf16[1,2048,256]{2,1,0:T(8,128)(2,1)} %param.39) | copy-start | bytes 3145732
  28.0 52.6 %collective-permute-start.4 = (bf16[2048,256]{1,0:T(8,128)(2,1)}, bf16[2048,256]{1,0:T(8,128)(2,1)}, u32[]{:S(2)}, u32[]{:S(2)}) collective-permute-start(bf16[2048,256]{1,0:T(8,128)(2,1)} %bitcast.9.g0), channel_id=1, source_target_pairs={{0,1},{1,2},{2,3},{3,0},{4,5},{5,6},{6,7},{7,4},{8,9},{9,10},{10,1... | collective-permute-start | bytes 3145736 | tf_op jit(solution)/shard_map/ppermute | solution.py:34
  29.6 51.2 %collective-permute-start.7 = (bf16[2048,256]{1,0:T(8,128)(2,1)}, bf16[2048,256]{1,0:T(8,128)(2,1)}, u32[]{:S(2)}, u32[]{:S(2)}) collective-permute-start(bf16[2048,256]{1,0:T(8,128)(2,1)} %bitcast.23), channel_id=1, source_target_pairs={{0,3},{1,0},{2,1},{3,2},{4,7},{5,4},{6,5},{7,6},{8,11},{9,8},{10,9... | collective-permute-start | bytes 3145736 | tf_op jit(solution)/shard_map/ppermute | solution.py:34
  31.4 35.4 %collective-permute-start.8 = (bf16[128,2048]{1,0:T(8,128)(2,1)S(1)}, bf16[128,2048]{1,0:T(8,128)(2,1)}, u32[]{:S(2)}, u32[]{:S(2)}) collective-permute-start(bf16[128,2048]{1,0:T(8,128)(2,1)S(1)} %get-tuple-element.29), channel_id=1, source_target_pairs={{0,1},{1,2},{2,3},{3,0},{4,5},{5,6},{6,7},{7,4},{8,9},{9,10},{10,1... | collective-permute-start | bytes 1572872 | tf_op jit(solution)/shard_map/ppermute | solution.py:34
  31.9 46.1 %collective-permute-start.9 = (bf16[128,2048]{1,0:T(8,128)(2,1)S(1)}, bf16[128,2048]{1,0:T(8,128)(2,1)S(1)}, u32[]{:S(2)}, u32[]{:S(2)}) collective-permute-start(bf16[128,2048]{1,0:T(8,128)(2,1)S(1)} %get-tuple-element.28), channel_id=1, source_target_pairs={{0,1},{1,2},{2,3},{3,0},{4,5},{5,6},{6,7},{7,4},{8,9},{9,10},{10,1... | collective-permute-start | bytes 1572872 | tf_op jit(solution)/shard_map/ppermute | solution.py:34
  33.4 50.4 %collective-permute-start.10 = (bf16[128,2048]{1,0:T(8,128)(2,1)S(1)}, bf16[128,2048]{1,0:T(8,128)(2,1)S(1)}, u32[]{:S(2)}, u32[]{:S(2)}) collective-permute-start(bf16[128,2048]{1,0:T(8,128)(2,1)S(1)} %get-tuple-element.29), channel_id=1, source_target_pairs={{0,3},{1,0},{2,1},{3,2},{4,7},{5,4},{6,5},{7,6},{8,11},{9,8},{10,9... | collective-permute-start | bytes 1572872 | tf_op jit(solution)/shard_map/ppermute | solution.py:34
  66.9 69.8 %collective-permute-start.5 = (bf16[2048,256]{1,0:T(8,128)(2,1)S(1)}, bf16[2048,256]{1,0:T(8,128)(2,1)S(1)}, u32[]{:S(2)}, u32[]{:S(2)}) collective-permute-start(bf16[2048,256]{1,0:T(8,128)(2,1)S(1)} %bitcast.24), channel_id=1, source_target_pairs={{0,1},{1,2},{2,3},{3,0},{4,5},{5,6},{6,7},{7,4},{8,9},{9,10},{10,1... | collective-permute-start | bytes 3145736 | tf_op jit(solution)/shard_map/ppermute | solution.py:34
  78.0 0.8 copy-start.10
  78.8 74.0 %collective-permute-start.6 = (bf16[2048,256]{1,0:T(8,128)(2,1)}, bf16[2048,256]{1,0:T(8,128)(2,1)}, u32[]{:S(2)}, u32[]{:S(2)}) collective-permute-start(bf16[2048,256]{1,0:T(8,128)(2,1)} %bitcast.9.g0), channel_id=1, source_target_pairs={{0,3},{1,0},{2,1},{3,2},{4,7},{5,4},{6,5},{7,6},{8,11},{9,8},{10,9... | collective-permute-start | bytes 3145736 | tf_op jit(solution)/shard_map/ppermute | solution.py:34
  80.6 83.4 %collective-permute-start.12 = (bf16[2048,256]{1,0:T(8,128)(2,1)}, bf16[2048,256]{1,0:T(8,128)(2,1)}, u32[]{:S(2)}, u32[]{:S(2)}) collective-permute-start(bf16[2048,256]{1,0:T(8,128)(2,1)} %collective-permute-done.4.g1), channel_id=1, source_target_pairs={{0,1},{1,2},{2,3},{3,0},{4,5},{5,6},{6,7},{7,4},{8,9},{9,10},{10,1... | collective-permute-start | bytes 3145736 | tf_op jit(solution)/shard_map/ppermute | solution.py:34
  80.8 83.1 %collective-permute-start.13 = (bf16[2048,256]{1,0:T(8,128)(2,1)}, bf16[2048,256]{1,0:T(8,128)(2,1)}, u32[]{:S(2)}, u32[]{:S(2)}) collective-permute-start(bf16[2048,256]{1,0:T(8,128)(2,1)} %collective-permute-done.7.u2), channel_id=1, source_target_pairs={{0,3},{1,0},{2,1},{3,2},{4,7},{5,4},{6,5},{7,6},{8,11},{9,8},{10,9... | collective-permute-start | bytes 3145736 | tf_op jit(solution)/shard_map/ppermute | solution.py:34
  83.8 0.8 copy-start.12
  84.6 51.8 %collective-permute-start.11 = (bf16[128,2048]{1,0:T(8,128)(2,1)S(1)}, bf16[128,2048]{1,0:T(8,128)(2,1)}, u32[]{:S(2)}, u32[]{:S(2)}) collective-permute-start(bf16[128,2048]{1,0:T(8,128)(2,1)S(1)} %get-tuple-element.28), channel_id=1, source_target_pairs={{0,3},{1,0},{2,1},{3,2},{4,7},{5,4},{6,5},{7,6},{8,11},{9,8},{10,9... | collective-permute-start | bytes 1572872 | tf_op jit(solution)/shard_map/ppermute | solution.py:34
  136.4 30.1 %collective-permute-start.14 = (bf16[128,2048]{1,0:T(8,128)(2,1)}, bf16[128,2048]{1,0:T(8,128)(2,1)}, u32[]{:S(2)}, u32[]{:S(2)}) collective-permute-start(bf16[128,2048]{1,0:T(8,128)(2,1)} %collective-permute-done.8.d1a), channel_id=1, source_target_pairs={{0,1},{1,2},{2,3},{3,0},{4,5},{5,6},{6,7},{7,4},{8,9},{9,10},{10,1... | collective-permute-start | bytes 1572872 | tf_op jit(solution)/shard_map/ppermute | solution.py:34
  136.7 1.0 copy-start.4
  137.7 28.8 %collective-permute-start.15 = (bf16[128,2048]{1,0:T(8,128)(2,1)}, bf16[128,2048]{1,0:T(8,128)(2,1)}, u32[]{:S(2)}, u32[]{:S(2)}) collective-permute-start(bf16[128,2048]{1,0:T(8,128)(2,1)} %collective-permute-done.11.d2b), channel_id=1, source_target_pairs={{0,3},{1,0},{2,1},{3,2},{4,7},{5,4},{6,5},{7,6},{8,11},{9,8},{10,9... | collective-permute-start | bytes 1572872 | tf_op jit(solution)/shard_map/ppermute | solution.py:34
  142.5 29.0 %all-to-all-start.1 = ((bf16[64,16,128]{2,1,0:T(8,128)(2,1)}), bf16[64,16,128]{2,1,0:T(8,128)(2,1)S(1)}, u32[]{:S(2)}, u32[]{:S(2)}) async-start(bf16[64,16,128]{2,1,0:T(8,128)(2,1)} %bitcast.5), calls=%async_computation.1 | async-start | bytes 524288 | tf_op jit(solution)/shard_map/all_to_all | solution.py:537
  152.8 1.2 copy-start.3
  154.1 1.2 copy-start.5
  155.3 1.0 copy-start.11
  156.3 1.0 copy-start.13
  171.5 10.5 %copy-start.6 = (bf16[2048,128]{1,0:T(8,128)(2,1)S(1)}, bf16[2048,128]{1,0:T(8,128)(2,1)}, u32[]{:S(2)}) copy-start(bf16[2048,128]{1,0:T(8,128)(2,1)} %gate_ref.3) | copy-start | bytes 1572868
  171.5 10.5 %copy-start.7 = (bf16[2048,128]{1,0:T(8,128)(2,1)S(1)}, bf16[2048,128]{1,0:T(8,128)(2,1)}, u32[]{:S(2)}) copy-start(bf16[2048,128]{1,0:T(8,128)(2,1)} %up_ref.1) | copy-start | bytes 1572868
  171.6 72.4 %all-to-all-start.2 = ((bf16[64,96,128]{2,1,0:T(8,128)(2,1)}), bf16[64,96,128]{2,1,0:T(8,128)(2,1)S(1)}, u32[]{:S(2)}, u32[]{:S(2)}) async-start(bf16[64,96,128]{2,1,0:T(8,128)(2,1)} %bitcast.27), calls=%async_computation.2 | async-start | bytes 3145728 | tf_op jit(solution)/shard_map/all_to_all | solution.py:585
  182.0 1.0 copy-start.8
  183.6 21.1 %collective-permute-start.17 = (bf16[3072,128]{1,0:T(8,128)(2,1)S(1)}, bf16[3072,128]{1,0:T(8,128)(2,1)S(1)}, u32[]{:S(2)}, u32[]{:S(2)}) collective-permute-start(bf16[3072,128]{1,0:T(8,128)(2,1)S(1)} %shared_pack.1.own), channel_id=1, source_target_pairs={{0,1},{1,2},{2,3},{3,0},{4,5},{5,6},{6,7},{7,4},{8,9},{9,10},{10,1... | collective-permute-start | bytes 2359304 | tf_op jit(solution)/shard_map/ppermute | solution.py:34
  183.9 23.0 %collective-permute-start.18 = (bf16[3072,128]{1,0:T(8,128)(2,1)S(1)}, bf16[3072,128]{1,0:T(8,128)(2,1)S(1)}, u32[]{:S(2)}, u32[]{:S(2)}) collective-permute-start(bf16[3072,128]{1,0:T(8,128)(2,1)S(1)} %shared_pack.1.own), channel_id=1, source_target_pairs={{0,3},{1,0},{2,1},{3,2},{4,7},{5,4},{6,5},{7,6},{8,11},{9,8},{10,9... | collective-permute-start | bytes 2359304 | tf_op jit(solution)/shard_map/ppermute | solution.py:34
  204.6 19.9 %collective-permute-start.19 = (bf16[3072,128]{1,0:T(8,128)(2,1)S(1)}, bf16[3072,128]{1,0:T(8,128)(2,1)S(1)}, u32[]{:S(2)}, u32[]{:S(2)}) collective-permute-start(bf16[3072,128]{1,0:T(8,128)(2,1)S(1)} %collective-permute-done.17.low), channel_id=1, source_target_pairs={{0,1},{1,2},{2,3},{3,0},{4,5},{5,6},{6,7},{7,4},{8,9},{9,10},{10,1... | collective-permute-start | bytes 2359304 | tf_op jit(solution)/shard_map/ppermute | solution.py:34
  204.6 23.8 %copy-start.21 = (s32[128,2]{0,1:T(2,128)S(1)}, s32[128,2]{0,1:T(2,128)}, u32[]{:S(2)}) copy-start(s32[128,2]{0,1:T(2,128)} %param.36) | copy-start | bytes 3076
  204.6 23.9 %copy-start.22 = (bf16[128,2]{0,1:T(2,128)(2,1)S(1)}, bf16[128,2]{0,1:T(2,128)(2,1)}, u32[]{:S(2)}) copy-start(bf16[128,2]{0,1:T(2,128)(2,1)} %param.37) | copy-start | bytes 1540
  204.6 24.1 %copy-start.9 = (f32[128,1024]{1,0:T(8,128)S(1)}, f32[128,1024]{1,0:T(8,128)}, u32[]{:S(2)}) copy-start(f32[128,1024]{1,0:T(8,128)} %get-tuple-element.18.local_ref) | copy-start | bytes 1572868
  204.6 2.2 collective-permute-start.16
  224.5 1.0 copy-start.14
  225.6 3.1 %copy-start.15 = (bf16[128,1024]{1,0:T(8,128)(2,1)S(1)}, bf16[128,1024]{1,0:T(8,128)(2,1)}, u32[]{:S(2)}) copy-start(bf16[128,1024]{1,0:T(8,128)(2,1)} %gate_ref.2) | copy-start | bytes 786436
  225.6 3.1 %copy-start.16 = (f32[128,128]{1,0:T(8,128)S(1)}, f32[128,128]{1,0:T(8,128)}, u32[]{:S(2)}) copy-start(f32[128,128]{1,0:T(8,128)} %get-tuple-element.16.read_ref) | copy-start | bytes 196612
  225.6 3.1 %copy-start.17 = (f32[128,16]{1,0:T(8,128)S(1)}, f32[128,16]{1,0:T(8,128)}, u32[]{:S(2)}) copy-start(f32[128,16]{1,0:T(8,128)} %get-tuple-element.17.grow_ref) | copy-start | bytes 24580
  225.6 3.1 %copy-start.18 = (f32[1024]{0:T(1024)S(1)}, f32[1024]{0:T(1024)}, u32[]{:S(2)}) copy-start(f32[1024]{0:T(1024)} %param.32) | copy-start | bytes 12292
  228.4 6.5 %collective-permute-start.20 = (bf16[128,2048]{1,0:T(8,128)(2,1)}, bf16[128,2048]{1,0:T(8,128)(2,1)}, u32[]{:S(2)}, u32[]{:S(2)}) collective-permute-start(bf16[128,2048]{1,0:T(8,128)(2,1)} %get-tuple-element.27), channel_id=1, source_target_pairs={{0,4},{4,0},{1,5},{5,1},{2,6},{6,2},{3,7},{7,3},{8,12},{12,8},{9,1... | collective-permute-start | bytes 1572872 | tf_op jit(solution)/shard_map/ppermute | solution.py:34
  228.7 2.2 copy-start
  230.9 4.0 %copy-start.19 = (f32[128,2048]{1,0:T(8,128)S(1)}, f32[128,2048]{1,0:T(8,128)}, u32[]{:S(2)}) copy-start(f32[128,2048]{1,0:T(8,128)} %get-tuple-element.26) | copy-start | bytes 3145732
  232.8 6.4 %collective-permute-start.3 = (bf16[32,2048]{1,0:T(8,128)(2,1)S(1)}, bf16[32,2048]{1,0:T(8,128)(2,1)S(1)}, u32[]{:S(2)}, u32[]{:S(2)}) collective-permute-start(bf16[32,2048]{1,0:T(8,128)(2,1)S(1)} %get-tuple-element.22), channel_id=1, source_target_pairs={{0,3},{1,0},{2,1},{3,2},{4,7},{5,4},{6,5},{7,6},{8,11},{9,8},{10,9... | collective-permute-start | bytes 393224 | tf_op jit(solution)/shard_map/ppermute | solution.py:34
  232.9 8.0 %collective-permute-start.2 = (bf16[32,2048]{1,0:T(8,128)(2,1)S(1)}, bf16[32,2048]{1,0:T(8,128)(2,1)S(1)}, u32[]{:S(2)}, u32[]{:S(2)}) collective-permute-start(bf16[32,2048]{1,0:T(8,128)(2,1)S(1)} %get-tuple-element.21), channel_id=1, source_target_pairs={{0,2},{1,3},{2,0},{3,1},{4,6},{5,7},{6,4},{7,5},{8,10},{9,11},{10,... | collective-permute-start | bytes 393224 | tf_op jit(solution)/shard_map/ppermute | solution.py:34
  234.1 9.2 %collective-permute-start.1 = (bf16[32,2048]{1,0:T(8,128)(2,1)S(1)}, bf16[32,2048]{1,0:T(8,128)(2,1)S(1)}, u32[]{:S(2)}, u32[]{:S(2)}) collective-permute-start(bf16[32,2048]{1,0:T(8,128)(2,1)S(1)} %get-tuple-element.20), channel_id=1, source_target_pairs={{0,1},{1,2},{2,3},{3,0},{4,5},{5,6},{6,7},{7,4},{8,9},{9,10},{10,1... | collective-permute-start | bytes 393224 | tf_op jit(solution)/shard_map/ppermute | solution.py:34
